TPU v7x, 128 devices: a whole 4x4x4 slice. The times are simulated.
128 devices in a mesh: sp: 16 (over z, y), tp: 8 (over x, core).
Axes of the slice: x: 4, y: 4, z: 4, core: 2. Of those that a mesh axis runs over, the one named last changes fastest.
Arguments:
- tokens: bfloat16 [16384, 2048], P('sp'), may hold values from -6 to 6
- norm_gain: float32 [2048], replicated, may hold values from 0.1 to 1.9
- attn_query: bfloat16 [2048, 1024], P(None, 'tp'), may hold values from -0.088388348 to 0.088388348
- attn_key: bfloat16 [2048, 1024], P(None, 'tp'), may hold values from -0.088388348 to 0.088388348
- attn_value: bfloat16 [2048, 1024], P(None, 'tp'), may hold values from -0.125 to 0.125
- score_scale: float32 [16], replicated, may hold values from 0.5 to 40
- attention_decay: float32 [16, 16384], P('tp'), as said below
- mem_query: bfloat16 [2048, 1024], P(None, 'tp'), may hold values from -0.125 to 0.125
- mem_key: bfloat16 [2048, 1024], P(None, 'tp'), may hold values from -0.125 to 0.125
- mem_value: bfloat16 [2048, 1024], P(None, 'tp'), may hold values from -0.125 to 0.125
- mem_ingate: bfloat16 [2048, 8], replicated, may hold values from -0.125 to 0.125
- input_shift: float32 [8], replicated, may hold values from -3 to 100
- memory_decay: float32 [8, 16384], P('tp', 'sp'), may hold values from -1.5 to 0
- mem_outgate: bfloat16 [2048, 1024], P(None, 'tp'), may hold values from -0.125 to 0.125
- init_memory: float32 [8, 128, 128], P('tp'), may hold values from -192 to 192
- init_normalizer: float32 [8, 128], P('tp'), may hold values from -192 to 192
- attn_gain: float32 [1024], replicated, may hold values from 0.1 to 1.9
- mem_gain: float32 [1024], replicated, may hold values from 0.1 to 1.9
- attn_out: bfloat16 [1024, 2048], replicated, may hold values from -0.125 to 0.125
- mem_out: bfloat16 [1024, 2048], replicated, may hold values from -0.125 to 0.125
Outputs:
- mixed: bfloat16 [16384, 2048], P(('sp', 'tp'))
Inputs may be any that keep to these rules, and one draw needn't show every extreme that they name: `attention_decay`: each head's row never rises from one position to the next.
All inputs are finite; a program needn't handle non-finite values.
Results may differ from a plain program's by a relative error of at most 0.025.
The roundings to bfloat16 on the way count: a program that leaves them out, or rounds other values in their place, can miss the bound.
Values may be sent and summed in bfloat16 or wider, within the bound.
A program may use at most 128 MiB of HBM per device.

v0:
```python
import math

import jax
import jax.numpy as jnp
from jax import lax
from jax.sharding import PartitionSpec as P

AHEADS = 16
ADIM = 64
MHEADS = 8
MDIM = 128
BLOCK = 128


epsilon = 1e-06
highest = lax.Precision.HIGHEST
far_below = -1e30


def in_one_piece(arrays, axis, dim, along):
    widths = [a.shape[along] for a in arrays]
    both = jnp.concatenate(arrays, axis=along)
    out = lax.all_gather(both, axis, axis=dim, tiled=True)
    return tuple(jnp.split(out, [sum(widths[:k]) for k in range(1, len(widths))], axis=along))


def in_order(blocks, dim):
    shape = list(blocks.shape[1:])
    shape[dim] *= blocks.shape[0]
    return jnp.moveaxis(blocks, 0, dim).reshape(shape)


def sent_to_all(value, axis):
    devices = lax.axis_size(axis)
    return lax.all_to_all(
        jnp.broadcast_to(value[None], (devices, *value.shape)), axis, 0, 0, tiled=True
    )


def gathered_copies(value, axis, dim):
    return in_order(sent_to_all(value, axis), dim)


def sent_together(arrays, axis, dim, along):
    widths = [math.prod(a.shape[along:]) for a in arrays]
    both = jnp.concatenate(
        [a.reshape(*a.shape[:along], w) for a, w in zip(arrays, widths)], axis=along
    )
    out = gathered_copies(both, axis, dim)
    blocks = jnp.split(out, [sum(widths[:k]) for k in range(1, len(widths))], axis=along)
    return tuple((b.reshape(*out.shape[:along], *a.shape[along:]) for a, b in zip(arrays, blocks)))


def taken_together(value, axis):
    return sent_to_all(value, axis).sum(axis=0)


def in_one(arrays, axis):
    ravelled, at, gathered = (jnp.concatenate([a.reshape(-1) for a in arrays]), 0, [])
    so_far = taken_together(ravelled, axis)
    for a in arrays:
        gathered.append(so_far[at : at + a.size].reshape(a.shape))
        at += a.size
    return tuple(gathered)


def rms_scale(values):
    return values * lax.rsqrt(jnp.mean(values * values, axis=-1, keepdims=True) + epsilon)


def advance(running, inputs):
    memory, normalizer, stabilizer = running
    block_memory, block_norm, block_top, decay_total = inputs
    new_stab = jnp.maximum(decay_total + stabilizer, block_top)
    shrink = jnp.exp(decay_total + stabilizer - new_stab)
    growth = jnp.exp(block_top - new_stab)
    memory_new = shrink[:, None, None] * memory + growth[:, None, None] * block_memory
    norm_new = shrink[:, None] * normalizer + growth[:, None] * block_norm
    return ((memory_new, norm_new, new_stab), (memory, normalizer, stabilizer))


def block_output(
    q_blocks, k_blocks, v_blocks, forget_cum, gate_blocks, mem_prev, norm_prev, stab_prev
):
    block_len = q_blocks.shape[-2]
    causal = jnp.tril(jnp.ones((block_len, block_len), dtype=bool))
    log_pair = jnp.where(
        causal,
        forget_cum[..., :, None] - forget_cum[..., None, :] + gate_blocks[..., None, :],
        -jnp.inf,
    )
    carried_log = forget_cum + stab_prev[..., None]
    row_top = jnp.maximum(carried_log, jnp.max(log_pair, axis=-1))
    pair_weight = jnp.einsum("hcld,hcsd->hcls", q_blocks, k_blocks, precision=highest) * jnp.exp(
        log_pair - row_top[..., None]
    )
    carried_weight = jnp.exp(carried_log - row_top)
    numer = jnp.einsum("hcls,hcsd->hcld", pair_weight, v_blocks, precision=highest)
    numer = numer + carried_weight[..., None] * jnp.einsum(
        "hcld,hcde->hcle", q_blocks, mem_prev, precision=highest
    )
    denom = jnp.sum(pair_weight, axis=-1) + carried_weight * jnp.einsum(
        "hcld,hcd->hcl", q_blocks, norm_prev, precision=highest
    )
    return numer / jnp.maximum(jnp.abs(denom), jnp.exp(-row_top))[..., None]


def on_device(
    tokens,
    norm_gain,
    attn_query,
    attn_key,
    attn_value,
    score_scale,
    attention_decay,
    mem_query,
    mem_key,
    mem_value,
    mem_ingate,
    input_shift,
    memory_decay,
    mem_outgate,
    init_memory,
    init_normalizer,
    attn_gain,
    mem_gain,
    attn_out,
    mem_out,
):
    local_rows = tokens.shape[0]
    head_rank = lax.axis_index("tp")
    seq_rank = lax.axis_index("sp")
    att_width = attn_query.shape[1]
    mem_width = mem_query.shape[1]
    att_heads = att_width // ADIM
    mem_heads = mem_width // MDIM
    normed = (rms_scale(tokens.astype(jnp.float32)) * norm_gain).astype(jnp.bfloat16)
    stacked = jnp.concatenate(
        [attn_query, attn_key, attn_value, mem_query, mem_key, mem_value, mem_outgate], axis=1
    )
    projected = jnp.dot(normed, stacked, preferred_element_type=jnp.float32).astype(jnp.bfloat16)
    query_hat = rms_scale(
        projected[:, :att_width].astype(jnp.float32).reshape(local_rows, att_heads, ADIM)
    ).astype(jnp.bfloat16)
    key_hat = (
        rms_scale(
            projected[:, att_width : 2 * att_width]
            .astype(jnp.float32)
            .reshape(local_rows, att_heads, ADIM)
        )
        .astype(jnp.bfloat16)
        .reshape(local_rows, att_width)
    )
    value_rows = projected[:, 2 * att_width : 3 * att_width]
    head_scale = lax.dynamic_slice_in_dim(score_scale, head_rank * att_heads, att_heads) * ADIM ** (
        -0.5
    )
    query_decay = lax.dynamic_slice_in_dim(attention_decay, seq_rank * local_rows, local_rows, 1)
    query_pos = seq_rank * local_rows + jnp.arange(local_rows, dtype=jnp.int32)
    groups = ((query_hat, query_decay, query_pos),)

    def fold_group(status, group, key_piece, value_piece):
        group_query, group_decay, group_pos = group
        group_last = group_pos[-1]
        piece_rows = key_piece.shape[0]
        shards_here = max(1, piece_rows // local_rows)
        reach = max(1, 1024 // local_rows)
        together = max(
            (
                count
                for count in range(1, shards_here + 1)
                if shards_here % count == 0 and count <= reach
            )
        )
        span_rows = min(piece_rows, together * local_rows)
        block_count = piece_rows // span_rows

        def visit(block_index, current_state):
            key_start = block_index * span_rows

            def update(current):
                row_best, totals, summed = current
                key_block = lax.dynamic_slice_in_dim(
                    key_piece, block_index * span_rows, span_rows, 0
                ).reshape(span_rows, att_heads, ADIM)
                value_block = lax.dynamic_slice_in_dim(
                    value_piece, block_index * span_rows, span_rows, 0
                ).reshape(span_rows, att_heads, ADIM)
                key_decay = lax.dynamic_slice_in_dim(attention_decay, key_start, span_rows, 1)
                scores = jnp.einsum(
                    "qhd,khd->hqk", group_query, key_block, preferred_element_type=jnp.float32
                )
                scores = (
                    scores * head_scale[:, None, None]
                    + group_decay[:, :, None]
                    - key_decay[:, None, :]
                )
                key_pos = key_start + jnp.arange(span_rows, dtype=jnp.int32)
                visible = (key_pos[None, :] <= group_pos[:, None])[None]
                masked = jnp.where(visible, scores, far_below)
                new_best = jnp.maximum(row_best, jnp.max(masked, axis=-1))
                weights = jnp.where(visible, jnp.exp(masked - new_best[..., None]), 0.0)
                rescale = jnp.exp(row_best - new_best)
                product = jnp.einsum(
                    "hqk,khd->hqd",
                    weights.astype(jnp.bfloat16),
                    value_block,
                    preferred_element_type=jnp.float32,
                )
                return (
                    new_best,
                    totals * rescale + jnp.sum(weights, axis=-1),
                    summed * rescale[..., None] + product,
                )

            return lax.cond(
                key_start <= group_last, update, lambda unchanged: unchanged, current_state
            )

        return lax.fori_loop(0, block_count, visit, status)

    start_fold = tuple(
        (
            (
                jnp.full((att_heads, group[2].shape[0]), far_below, jnp.float32),
                jnp.zeros((att_heads, group[2].shape[0]), jnp.float32),
                jnp.zeros((att_heads, group[2].shape[0], ADIM), jnp.float32),
            )
            for group in groups
        )
    )
    key_piece, value_piece = in_one_piece((key_hat, value_rows), "sp", 0, 1)
    folded = tuple(
        (
            fold_group(status, group, key_piece, value_piece)
            for status, group in zip(start_fold, groups)
        )
    )
    results = [
        (group_state[2] / group_state[1][..., None]).transpose(1, 0, 2) for group_state in folded
    ]
    attended = results[0].reshape(local_rows, att_width)
    mem_base = 3 * att_width
    block_count = local_rows // BLOCK

    def mem_heads_first(first_col):
        part_rows = projected[:, first_col : first_col + mem_width].astype(jnp.float32)
        return (
            part_rows.reshape(local_rows, mem_heads, MDIM)
            .transpose(1, 0, 2)
            .reshape(mem_heads, block_count, BLOCK, MDIM)
        )

    mem_queries = mem_heads_first(mem_base) * MDIM ** (-0.5)
    mem_keys = mem_heads_first(mem_base + mem_width)
    mem_values = mem_heads_first(mem_base + 2 * mem_width)
    gate_cols = lax.dynamic_slice_in_dim(mem_ingate, head_rank * mem_heads, mem_heads, 1)
    shift_part = lax.dynamic_slice_in_dim(input_shift, head_rank * mem_heads, mem_heads)
    in_gate = (
        jnp.dot(normed, gate_cols, preferred_element_type=jnp.float32) + shift_part
    ).T.reshape(mem_heads, block_count, BLOCK)
    forget_cum = jnp.cumsum(memory_decay.reshape(mem_heads, block_count, BLOCK), axis=-1)
    weight_log = forget_cum[..., -1:] - forget_cum + in_gate
    block_top = jnp.max(weight_log, axis=-1)
    scaled = jnp.exp(weight_log - block_top[..., None])
    block_memory = jnp.einsum(
        "hcl,hcld,hcle->hcde", scaled, mem_keys, mem_values, precision=highest
    )
    block_norm = jnp.einsum("hcl,hcld->hcd", scaled, mem_keys, precision=highest)
    block_decay = forget_cum[..., -1]
    sequence_inputs = (
        jnp.moveaxis(block_memory, 1, 0),
        jnp.moveaxis(block_norm, 1, 0),
        jnp.moveaxis(block_top, 1, 0),
        jnp.moveaxis(block_decay, 1, 0),
    )
    zero_state = (
        jnp.zeros((mem_heads, MDIM, MDIM), jnp.float32),
        jnp.zeros((mem_heads, MDIM), jnp.float32),
        jnp.zeros((mem_heads,), jnp.float32),
    )
    (own_memory, own_norm, own_stab), _ = lax.scan(advance, zero_state, sequence_inputs)
    decay_sum = jnp.sum(block_decay, axis=-1)
    all_memory, all_norm, all_stab, all_decay = sent_together(
        (own_memory[None], own_norm[None], own_stab[None], decay_sum[None]), "sp", 0, 2
    )
    source_count = all_decay.shape[0]
    source_index = jnp.arange(source_count, dtype=jnp.int32)
    earlier = source_index < seq_rank
    between = (source_index[None, :] > source_index[:, None]) & earlier[None, :]
    later_decay = jnp.dot(between.astype(jnp.float32), all_decay, precision=highest)
    before_total = jnp.sum(jnp.where(earlier[:, None], all_decay, 0.0), axis=0)
    source_log = jnp.where(earlier[:, None], all_stab + later_decay, far_below)
    joined = jnp.maximum(before_total, jnp.max(source_log, axis=0))
    source_weight = jnp.where(earlier[:, None], jnp.exp(source_log - joined[None, :]), 0.0)
    start_weight = jnp.exp(before_total - joined)
    entering_memory = start_weight[:, None, None] * init_memory + jnp.einsum(
        "sh,shde->hde", source_weight, all_memory, precision=highest
    )
    entering_norm = start_weight[:, None] * init_normalizer + jnp.einsum(
        "sh,shd->hd", source_weight, all_norm, precision=highest
    )
    entering = (entering_memory, entering_norm, joined)
    _, (mem_prev, norm_prev, stab_prev) = lax.scan(
        advance, (entering[0], entering[1], entering[2]), sequence_inputs
    )
    mem_prev = jnp.moveaxis(mem_prev, 0, 1)
    norm_prev = jnp.moveaxis(norm_prev, 0, 1)
    stab_prev = jnp.moveaxis(stab_prev, 0, 1)
    recalled = block_output(
        mem_queries, mem_keys, mem_values, forget_cum, in_gate, mem_prev, norm_prev, stab_prev
    )
    recalled = (
        recalled.reshape(mem_heads, local_rows, MDIM)
        .transpose(1, 0, 2)
        .reshape(local_rows, mem_width)
    )
    att_squares, mem_squares = in_one(
        (jnp.sum(attended * attended, axis=1), jnp.sum(recalled * recalled, axis=1)), "tp"
    )
    att_factor = lax.rsqrt(att_squares / (AHEADS * ADIM) + epsilon)
    mem_factor = lax.rsqrt(mem_squares / (MHEADS * MDIM) + epsilon)
    att_gain_rows = lax.dynamic_slice_in_dim(attn_gain, head_rank * att_width, att_width)
    att_mix = (attended * att_factor[:, None] * att_gain_rows).astype(jnp.bfloat16)
    out_gate = jax.nn.sigmoid(projected[:, mem_base + 3 * mem_width :].astype(jnp.float32))
    mem_gain_rows = lax.dynamic_slice_in_dim(mem_gain, head_rank * mem_width, mem_width)
    mem_mix = (recalled * mem_factor[:, None] * mem_gain_rows * out_gate).astype(jnp.bfloat16)
    att_all, mem_all = (
        lax.all_to_all(att_mix, "tp", split_axis=0, concat_axis=1, tiled=True),
        lax.all_to_all(mem_mix, "tp", split_axis=0, concat_axis=1, tiled=True),
    )
    mixed = jnp.dot(att_all, attn_out, preferred_element_type=jnp.float32) + jnp.dot(
        mem_all, mem_out, preferred_element_type=jnp.float32
    )
    return mixed.astype(jnp.bfloat16)


def solution(mesh):
    placed = (
        P("sp", None),
        P(),
        P(None, "tp"),
        P(None, "tp"),
        P(None, "tp"),
        P(),
        P("tp", None),
        P(None, "tp"),
        P(None, "tp"),
        P(None, "tp"),
        P(),
        P(),
        P("tp", "sp"),
        P(None, "tp"),
        P("tp", None, None),
        P("tp", None),
        P(),
        P(),
        P(),
        P(),
    )
    return jax.shard_map(
        on_device, mesh=mesh, in_specs=placed, out_specs=P(("sp", "tp"), None), check_vma=False
    )
```

profile of v0, /device:TPU:120, one launch (start us, length us, event | category | flops | bytes accessed | tf_op | source)
XLA Modules:
  0.0 378.6 jit_solution(11542190993445788044)
XLA Ops:
  12.2 4.6 %convolution_convert_fusion = bf16[1024,896]{1,0:T(8,128)(2,1)S(1)} fusion(bf16[2048,896]{1,0:T(8,128)(2,1)S(1)} %constant_dynamic-update-slice_fusion.1, bf16[1024,2048]{1,0:T(8,128)(2,1)S(1)} %copy-done.2, f32[2048]{0:T(1024)S(1)} %copy-done.14, f32[1024]{0:T(1024)S(1)} %add_rsqrt_fusion.2), kind=kOutput, calls=%fused_computation.44 | convolution fusion | flops 3767402496 | bytes 9711616 | tf_op jit(solution)/shard_map/dot_general | solution.py:141
  23.1 3.5 fusion.25
  30.7 20.3 %while.55 = (s32[]{:T(128)}, f32[1,128,128]{2,1,0:T(8,128)S(1)}, f32[1,128]{1,0:T(1,128)S(1)}, f32[1]{0:T(128)}, f32[8,1]{0,1:T(1,128)S(1)}, /*index=5*/f32[8,1]...) while((s32[]{:T(128)}, f32[1,128,128]{2,1,0:T(8,128)S(1)}, ...), condition=%wide.region_13.14_spmd.clone, body=%wide.region_12.13_spmd.clone.sunk | while | flops 66055 | bytes 198364 | solution.py:282
  53.5 7.0 %all-to-all-start = ((f32[16,1,1,16514]{3,2,1,0:T(1,128)}), f32[16,1,1,16514]{3,2,1,0:T(1,128)S(1)}, u32[]{:S(2)}, u32[]{:S(2)}) async-start(f32[16,1,1,16514]{3,2,1,0:T(1,128)} %broadcast_in_dim.143), calls=%async_computation | async-start | bytes 2129920 | tf_op jit(solution)/shard_map/all_to_all | solution.py:35
  64.4 21.7 %all-to-all-done = f32[16,1,1,16514]{3,2,1,0:T(1,128)S(1)} async-done(((f32[16,1,1,16514]{3,2,1,0:T(1,128)}), f32[16,1,1,16514]{3,2,1,0:T(1,128)S(1)}, u32[]{:S(2)}, u32[]{:S(2)}) %all-to-all-start) | async-done | bytes 1056928 | tf_op jit(solution)/shard_map/all_to_all | solution.py:35
  91.7 26.0 %while.53 = (s32[]{:T(128)}, f32[1,128,128]{2,1,0:T(8,128)S(1)}, f32[1,128]{1,0:T(1,128)S(1)}, f32[1]{0:T(128)}, f32[8,1,128,128]{3,2,1,0:T(8,128)}, /*index=5*/...) while((s32[]{:T(128)}, f32[1,128,128]{2,1,0:T(8,128)S(1)}, ...), condition=%wide.region_18.19_spmd, body=%wide.region_17.18_spmd.sunk | while | flops 49542 | bytes 331009 | solution.py:304
  122.0 5.7 %fusion.60 = (bf16[16384,128]{1,0:T(8,128)(2,1)}, bf16[16384,128]{1,0:T(8,128)(2,1)}) fusion(bf16[16384,256]{1,0:T(8,128)(2,1)} %all-gather.2.cloned.1.call-done), kind=kLoop, calls=%fused_computation.130 | loop fusion | bytes 16777216 | tf_op jit(solution)/shard_map/split | solution.py:24
  127.8 6.4 %copy.100 = bf16[16384,128]{0,1:T(8,128)(2,1)} copy(bf16[16384,128]{1,0:T(8,128)(2,1)} %get-tuple-element.728) | data formatting | bytes 8388608
  134.2 6.4 %copy.99 = bf16[16384,128]{0,1:T(8,128)(2,1)} copy(bf16[16384,128]{1,0:T(8,128)(2,1)} %get-tuple-element.729) | data formatting | bytes 8388608
  140.6 194.0 %while.54 = (s32[]{:T(128)}, f32[2,1024]{1,0:T(2,128)S(1)}, f32[2,1024]{1,0:T(2,128)S(1)}, f32[2,1024,64]{1,2,0:T(8,128)S(1)}, s32[]{:T(128)}, /*index=5*/bf16[1...) while((s32[]{:T(128)}, f32[2,1024]{1,0:T(2,128)S(1)}, ...), condition=%wide.region_8.9_spmd.clone, body=%wide.region_3.8_spmd.clone.sunk | while | flops 578033664 | bytes 32465336 | solution.py:220
  141.5 11.4 %conditional.3 = ((f32[2,1024]{1,0:T(2,128)S(1)}, f32[2,1024]{1,0:T(2,128)S(1)}, f32[2,1024,64]{1,2,0:T(8,128)S(1)})) conditional(s32[]{:T(128)} %convert_element_type.91, (f32[2,1024]{1,0:T(2,128)S(1)}, f32[2,1024]{1,0:T(2,128)S(1)}, f32[2,1024,64]{1,2,0:T(8,128)S(1)}) %tuple.115, (s32[]{:T(128)}, s32[]{:T(128)}, s32[]{:T(128)}, ...), branch_computations={%region_4.0_spmd, %region_5.7_spmd} | conditional | flops 578033664 | bytes 32460952 | solution.py:216
  149.5 3.4 fusion.7
  153.6 11.4 %conditional.3 = ((f32[2,1024]{1,0:T(2,128)S(1)}, f32[2,1024]{1,0:T(2,128)S(1)}, f32[2,1024,64]{1,2,0:T(8,128)S(1)})) conditional(s32[]{:T(128)} %convert_element_type.91, (f32[2,1024]{1,0:T(2,128)S(1)}, f32[2,1024]{1,0:T(2,128)S(1)}, f32[2,1024,64]{1,2,0:T(8,128)S(1)}) %tuple.115, (s32[]{:T(128)}, s32[]{:T(128)}, s32[]{:T(128)}, ...), branch_computations={%region_4.0_spmd, %region_5.7_spmd} | conditional | flops 578033664 | bytes 32460952 | solution.py:216
  165.7 11.4 %conditional.3 = ((f32[2,1024]{1,0:T(2,128)S(1)}, f32[2,1024]{1,0:T(2,128)S(1)}, f32[2,1024,64]{1,2,0:T(8,128)S(1)})) conditional(s32[]{:T(128)} %convert_element_type.91, (f32[2,1024]{1,0:T(2,128)S(1)}, f32[2,1024]{1,0:T(2,128)S(1)}, f32[2,1024,64]{1,2,0:T(8,128)S(1)}) %tuple.115, (s32[]{:T(128)}, s32[]{:T(128)}, s32[]{:T(128)}, ...), branch_computations={%region_4.0_spmd, %region_5.7_spmd} | conditional | flops 578033664 | bytes 32460952 | solution.py:216
  177.9 11.4 %conditional.3 = ((f32[2,1024]{1,0:T(2,128)S(1)}, f32[2,1024]{1,0:T(2,128)S(1)}, f32[2,1024,64]{1,2,0:T(8,128)S(1)})) conditional(s32[]{:T(128)} %convert_element_type.91, (f32[2,1024]{1,0:T(2,128)S(1)}, f32[2,1024]{1,0:T(2,128)S(1)}, f32[2,1024,64]{1,2,0:T(8,128)S(1)}) %tuple.115, (s32[]{:T(128)}, s32[]{:T(128)}, s32[]{:T(128)}, ...), branch_computations={%region_4.0_spmd, %region_5.7_spmd} | conditional | flops 578033664 | bytes 32460952 | solution.py:216
  190.0 11.4 %conditional.3 = ((f32[2,1024]{1,0:T(2,128)S(1)}, f32[2,1024]{1,0:T(2,128)S(1)}, f32[2,1024,64]{1,2,0:T(8,128)S(1)})) conditional(s32[]{:T(128)} %convert_element_type.91, (f32[2,1024]{1,0:T(2,128)S(1)}, f32[2,1024]{1,0:T(2,128)S(1)}, f32[2,1024,64]{1,2,0:T(8,128)S(1)}) %tuple.115, (s32[]{:T(128)}, s32[]{:T(128)}, s32[]{:T(128)}, ...), branch_computations={%region_4.0_spmd, %region_5.7_spmd} | conditional | flops 578033664 | bytes 32460952 | solution.py:216
  202.1 11.4 %conditional.3 = ((f32[2,1024]{1,0:T(2,128)S(1)}, f32[2,1024]{1,0:T(2,128)S(1)}, f32[2,1024,64]{1,2,0:T(8,128)S(1)})) conditional(s32[]{:T(128)} %convert_element_type.91, (f32[2,1024]{1,0:T(2,128)S(1)}, f32[2,1024]{1,0:T(2,128)S(1)}, f32[2,1024,64]{1,2,0:T(8,128)S(1)}) %tuple.115, (s32[]{:T(128)}, s32[]{:T(128)}, s32[]{:T(128)}, ...), branch_computations={%region_4.0_spmd, %region_5.7_spmd} | conditional | flops 578033664 | bytes 32460952 | solution.py:216
  214.2 11.4 %conditional.3 = ((f32[2,1024]{1,0:T(2,128)S(1)}, f32[2,1024]{1,0:T(2,128)S(1)}, f32[2,1024,64]{1,2,0:T(8,128)S(1)})) conditional(s32[]{:T(128)} %convert_element_type.91, (f32[2,1024]{1,0:T(2,128)S(1)}, f32[2,1024]{1,0:T(2,128)S(1)}, f32[2,1024,64]{1,2,0:T(8,128)S(1)}) %tuple.115, (s32[]{:T(128)}, s32[]{:T(128)}, s32[]{:T(128)}, ...), branch_computations={%region_4.0_spmd, %region_5.7_spmd} | conditional | flops 578033664 | bytes 32460952 | solution.py:216
  226.3 11.4 %conditional.3 = ((f32[2,1024]{1,0:T(2,128)S(1)}, f32[2,1024]{1,0:T(2,128)S(1)}, f32[2,1024,64]{1,2,0:T(8,128)S(1)})) conditional(s32[]{:T(128)} %convert_element_type.91, (f32[2,1024]{1,0:T(2,128)S(1)}, f32[2,1024]{1,0:T(2,128)S(1)}, f32[2,1024,64]{1,2,0:T(8,128)S(1)}) %tuple.115, (s32[]{:T(128)}, s32[]{:T(128)}, s32[]{:T(128)}, ...), branch_computations={%region_4.0_spmd, %region_5.7_spmd} | conditional | flops 578033664 | bytes 32460952 | solution.py:216
  238.4 11.4 %conditional.3 = ((f32[2,1024]{1,0:T(2,128)S(1)}, f32[2,1024]{1,0:T(2,128)S(1)}, f32[2,1024,64]{1,2,0:T(8,128)S(1)})) conditional(s32[]{:T(128)} %convert_element_type.91, (f32[2,1024]{1,0:T(2,128)S(1)}, f32[2,1024]{1,0:T(2,128)S(1)}, f32[2,1024,64]{1,2,0:T(8,128)S(1)}) %tuple.115, (s32[]{:T(128)}, s32[]{:T(128)}, s32[]{:T(128)}, ...), branch_computations={%region_4.0_spmd, %region_5.7_spmd} | conditional | flops 578033664 | bytes 32460952 | solution.py:216
  250.5 11.4 %conditional.3 = ((f32[2,1024]{1,0:T(2,128)S(1)}, f32[2,1024]{1,0:T(2,128)S(1)}, f32[2,1024,64]{1,2,0:T(8,128)S(1)})) conditional(s32[]{:T(128)} %convert_element_type.91, (f32[2,1024]{1,0:T(2,128)S(1)}, f32[2,1024]{1,0:T(2,128)S(1)}, f32[2,1024,64]{1,2,0:T(8,128)S(1)}) %tuple.115, (s32[]{:T(128)}, s32[]{:T(128)}, s32[]{:T(128)}, ...), branch_computations={%region_4.0_spmd, %region_5.7_spmd} | conditional | flops 578033664 | bytes 32460952 | solution.py:216
  262.6 11.4 %conditional.3 = ((f32[2,1024]{1,0:T(2,128)S(1)}, f32[2,1024]{1,0:T(2,128)S(1)}, f32[2,1024,64]{1,2,0:T(8,128)S(1)})) conditional(s32[]{:T(128)} %convert_element_type.91, (f32[2,1024]{1,0:T(2,128)S(1)}, f32[2,1024]{1,0:T(2,128)S(1)}, f32[2,1024,64]{1,2,0:T(8,128)S(1)}) %tuple.115, (s32[]{:T(128)}, s32[]{:T(128)}, s32[]{:T(128)}, ...), branch_computations={%region_4.0_spmd, %region_5.7_spmd} | conditional | flops 578033664 | bytes 32460952 | solution.py:216
  274.7 11.4 %conditional.3 = ((f32[2,1024]{1,0:T(2,128)S(1)}, f32[2,1024]{1,0:T(2,128)S(1)}, f32[2,1024,64]{1,2,0:T(8,128)S(1)})) conditional(s32[]{:T(128)} %convert_element_type.91, (f32[2,1024]{1,0:T(2,128)S(1)}, f32[2,1024]{1,0:T(2,128)S(1)}, f32[2,1024,64]{1,2,0:T(8,128)S(1)}) %tuple.115, (s32[]{:T(128)}, s32[]{:T(128)}, s32[]{:T(128)}, ...), branch_computations={%region_4.0_spmd, %region_5.7_spmd} | conditional | flops 578033664 | bytes 32460952 | solution.py:216
  286.8 11.4 %conditional.3 = ((f32[2,1024]{1,0:T(2,128)S(1)}, f32[2,1024]{1,0:T(2,128)S(1)}, f32[2,1024,64]{1,2,0:T(8,128)S(1)})) conditional(s32[]{:T(128)} %convert_element_type.91, (f32[2,1024]{1,0:T(2,128)S(1)}, f32[2,1024]{1,0:T(2,128)S(1)}, f32[2,1024,64]{1,2,0:T(8,128)S(1)}) %tuple.115, (s32[]{:T(128)}, s32[]{:T(128)}, s32[]{:T(128)}, ...), branch_computations={%region_4.0_spmd, %region_5.7_spmd} | conditional | flops 578033664 | bytes 32460952 | solution.py:216
  298.9 11.4 %conditional.3 = ((f32[2,1024]{1,0:T(2,128)S(1)}, f32[2,1024]{1,0:T(2,128)S(1)}, f32[2,1024,64]{1,2,0:T(8,128)S(1)})) conditional(s32[]{:T(128)} %convert_element_type.91, (f32[2,1024]{1,0:T(2,128)S(1)}, f32[2,1024]{1,0:T(2,128)S(1)}, f32[2,1024,64]{1,2,0:T(8,128)S(1)}) %tuple.115, (s32[]{:T(128)}, s32[]{:T(128)}, s32[]{:T(128)}, ...), branch_computations={%region_4.0_spmd, %region_5.7_spmd} | conditional | flops 578033664 | bytes 32460952 | solution.py:216
  311.1 11.4 %conditional.3 = ((f32[2,1024]{1,0:T(2,128)S(1)}, f32[2,1024]{1,0:T(2,128)S(1)}, f32[2,1024,64]{1,2,0:T(8,128)S(1)})) conditional(s32[]{:T(128)} %convert_element_type.91, (f32[2,1024]{1,0:T(2,128)S(1)}, f32[2,1024]{1,0:T(2,128)S(1)}, f32[2,1024,64]{1,2,0:T(8,128)S(1)}) %tuple.115, (s32[]{:T(128)}, s32[]{:T(128)}, s32[]{:T(128)}, ...), branch_computations={%region_4.0_spmd, %region_5.7_spmd} | conditional | flops 578033664 | bytes 32460952 | solution.py:216
  323.2 11.4 %conditional.3 = ((f32[2,1024]{1,0:T(2,128)S(1)}, f32[2,1024]{1,0:T(2,128)S(1)}, f32[2,1024,64]{1,2,0:T(8,128)S(1)})) conditional(s32[]{:T(128)} %convert_element_type.91, (f32[2,1024]{1,0:T(2,128)S(1)}, f32[2,1024]{1,0:T(2,128)S(1)}, f32[2,1024,64]{1,2,0:T(8,128)S(1)}) %tuple.115, (s32[]{:T(128)}, s32[]{:T(128)}, s32[]{:T(128)}, ...), branch_computations={%region_4.0_spmd, %region_5.7_spmd} | conditional | flops 578033664 | bytes 32460952 | solution.py:216
  335.4 4.3 %all-to-all-start.1 = ((f32[8,1,2048]{2,1,0:T(1,128)}), f32[8,1,2048]{2,1,0:T(1,128)S(1)}, u32[]{:S(2)}, u32[]{:S(2)}) async-start(f32[8,1,2048]{2,1,0:T(1,128)} %broadcast_in_dim.151), calls=%async_computation.1 | async-start | bytes 131072 | tf_op jit(solution)/shard_map/all_to_all | solution.py:35
  341.3 4.0 %all-to-all-done.1 = f32[8,1,2048]{2,1,0:T(1,128)S(1)} async-done(((f32[8,1,2048]{2,1,0:T(1,128)}), f32[8,1,2048]{2,1,0:T(1,128)S(1)}, u32[]{:S(2)}, u32[]{:S(2)}) %all-to-all-start.1) | async-done | bytes 65568 | tf_op jit(solution)/shard_map/all_to_all | solution.py:35
  351.8 5.4 %all-to-all-done.2 = bf16[8,128,128]{1,2,0:T(8,128)(2,1)S(1)} async-done(((bf16[8,128,128]{1,2,0:T(8,128)(2,1)}), bf16[8,128,128]{1,2,0:T(8,128)(2,1)S(1)}, u32[]{:S(2)}, u32[]{:S(2)}) %all-to-all-start.2) | async-done | bytes 262176 | tf_op jit(solution)/shard_map/all_to_all | solution.py:329
  363.5 4.5 %all-to-all-done.3 = bf16[8,128,128]{1,2,0:T(8,128)(2,1)S(1)} async-done(((bf16[8,128,128]{1,2,0:T(8,128)(2,1)}), bf16[8,128,128]{1,2,0:T(8,128)(2,1)S(1)}, u32[]{:S(2)}, u32[]{:S(2)}) %all-to-all-start.3) | async-done | bytes 262176 | tf_op jit(solution)/shard_map/all_to_all | solution.py:330
  368.0 3.7 fusion.22
  (361 shorter events, 239.9 us)
Async XLA Ops:
  6.5 16.6 %copy-start = (bf16[2048,8]{0,1:T(8,128)(2,1)S(1)}, bf16[2048,8]{0,1:T(8,128)(2,1)}, u32[]{:S(2)}) copy-start(bf16[2048,8]{0,1:T(8,128)(2,1)} %param.38) | copy-start | bytes 98308
  6.5 3.4 copy-start.4
  6.5 3.5 copy-start.5
  6.5 3.6 copy-start.6
  6.5 3.7 copy-start.7
  6.5 3.9 %copy-start.8 = (bf16[2048,128]{1,0:T(8,128)(2,1)S(1)}, bf16[2048,128]{1,0:T(8,128)(2,1)}, u32[]{:S(2)}) copy-start(bf16[2048,128]{1,0:T(8,128)(2,1)} %param.36) | copy-start | bytes 1572868
  6.6 4.0 %copy-start.9 = (bf16[2048,128]{1,0:T(8,128)(2,1)S(1)}, bf16[2048,128]{1,0:T(8,128)(2,1)}, u32[]{:S(2)}) copy-start(bf16[2048,128]{1,0:T(8,128)(2,1)} %param.37) | copy-start | bytes 1572868
  6.6 115.5 %all-gather.2.cloned.1.call-start = ((), (), s32[]{:S(2)}) async-start(), calls=%async_computation.4 | async-start | bytes 8912896 | tf_op jit(solution)/shard_map/all_gather | solution.py:23
  9.8 1.0 copy-start.10
  9.9 2.4 copy-start.2
  9.9 2.3 copy-start.14
  16.8 6.3 %copy-start.3 = (bf16[1024,896]{1,0:T(8,128)(2,1)}, bf16[1024,896]{1,0:T(8,128)(2,1)S(1)}, u32[]{:S(2)}) copy-start(bf16[1024,896]{1,0:T(8,128)(2,1)S(1)} %convolution_convert_fusion) | copy-start | bytes 5505028
  23.1 3.5 copy-start.15
  23.1 4.1 %copy-start.12 = (f32[1,1024]{1,0:T(1,128)S(1)}, f32[1,1024]{1,0:T(1,128)}, u32[]{:S(2)}) copy-start(f32[1,1024]{1,0:T(1,128)} %param.40) | copy-start | bytes 12292
  26.6 36.5 %copy-start.16 = (f32[16]{0:T(128)S(1)}, f32[16]{0:T(128)}, u32[]{:S(2)}) copy-start(f32[16]{0:T(128)} %param.33) | copy-start | bytes 196
  51.0 39.3 %copy-start.13 = (f32[1,128]{1,0:T(1,128)S(1)}, f32[1,128]{1,0:T(1,128)}, u32[]{:S(2)}) copy-start(f32[1,128]{1,0:T(1,128)} %param.43) | copy-start | bytes 1540
  53.5 38.1 %copy-start.11 = (f32[1,128,128]{2,1,0:T(8,128)S(1)}, f32[1,128,128]{2,1,0:T(8,128)}, u32[]{:S(2)}) copy-start(f32[1,128,128]{2,1,0:T(8,128)} %param.42) | copy-start | bytes 196612
  53.5 32.5 %all-to-all-start = ((f32[16,1,1,16514]{3,2,1,0:T(1,128)}), f32[16,1,1,16514]{3,2,1,0:T(1,128)S(1)}, u32[]{:S(2)}, u32[]{:S(2)}) async-start(f32[16,1,1,16514]{3,2,1,0:T(1,128)} %broadcast_in_dim.143), calls=%async_computation | async-start | bytes 2129920 | tf_op jit(solution)/shard_map/all_to_all | solution.py:35
  335.4 9.9 %all-to-all-start.1 = ((f32[8,1,2048]{2,1,0:T(1,128)}), f32[8,1,2048]{2,1,0:T(1,128)S(1)}, u32[]{:S(2)}, u32[]{:S(2)}) async-start(f32[8,1,2048]{2,1,0:T(1,128)} %broadcast_in_dim.151), calls=%async_computation.1 | async-start | bytes 131072 | tf_op jit(solution)/shard_map/all_to_all | solution.py:35
  346.3 10.9 %all-to-all-start.2 = ((bf16[8,128,128]{1,2,0:T(8,128)(2,1)}), bf16[8,128,128]{1,2,0:T(8,128)(2,1)S(1)}, u32[]{:S(2)}, u32[]{:S(2)}) async-start(bf16[8,128,128]{1,2,0:T(8,128)(2,1)} %copy.107), calls=%async_computation.2 | async-start | bytes 524288 | tf_op jit(solution)/shard_map/all_to_all | solution.py:329
  357.2 10.8 %all-to-all-start.3 = ((bf16[8,128,128]{1,2,0:T(8,128)(2,1)}), bf16[8,128,128]{1,2,0:T(8,128)(2,1)S(1)}, u32[]{:S(2)}, u32[]{:S(2)}) async-start(bf16[8,128,128]{1,2,0:T(8,128)(2,1)} %copy.108), calls=%async_computation.3 | async-start | bytes 524288 | tf_op jit(solution)/shard_map/all_to_all | solution.py:330
  360.6 11.2 %copy-start.1 = (bf16[2048,8]{0,1:T(8,128)(2,1)S(1)}, bf16[2048,8]{0,1:T(8,128)(2,1)}, u32[]{:S(2)}) copy-start(bf16[2048,8]{0,1:T(8,128)(2,1)} %param.38) | copy-start | bytes 98308
Sparse Core Ops, SparseCore 0:
  23.2 81.3 all-gather.1
where the time goes:
time: 381 us; the launch traced here: 379 us
  matrix products  116 us (30%)
  local copies, waits for them, and re-layouts  77 us (20%)
  other arithmetic  73.7 us (19%)
  loops' own time  42.5 us (11%)
  waiting for transfers between devices  35.6 us (9%)
  starting transfers between devices  18.1 us (5%)
  between operations  15.6 us (4%)
    dot_general x16, matrix products, update(): jnp.einsum('hqk,khd->hqd', weights.astype(jnp.bfloat16), value_block, pre...  54.9 us
    reduce_sum x16, other arithmetic, update(): jnp.sum(weights, axis=-1)  48.9 us
    dot_general x16, matrix products, update(): jnp.einsum('qhd,khd->hqk', group_query, key_block, preferred_element_type...  38.4 us
    all_to_all x2, waiting for transfers between devices, sent_to_all(): lax.all_to_all(jnp.broadcast_to(value[None], (devices, *value.shape)), ax...  25.7 us
    dynamic_slice x16, local copies, waits for them, and re-layouts, update(): lax.dynamic_slice_in_dim(value_piece, block_index * span_rows, span_rows, 0)  17.1 us
    another operation x1, loops' own time, on_device(): lax.scan(advance, zero_state, sequence_inputs)  15.2 us
    unnamed x43, local copies, waits for them, and re-layouts  15 us
    another operation x1, loops' own time, on_device(): lax.scan(advance, (entering[0], entering[1], entering[2]), sequence_inputs)  15 us
  transfers between devices with their start and end apart: 5, of which 4 were waited for; matrix products, arithmetic and copies ran while one was open for 12% of the time, Pallas kernels for 0%

commit v1 on v0

v1 whole, which is shorter than its diff:
```python
import functools
import math

import jax
import jax.numpy as jnp
from jax import lax
from jax.experimental import pallas as pl
from jax.experimental.pallas import tpu as pltpu
from jax.sharding import PartitionSpec as P

MESH = pl.DeviceIdType.MESH
f32 = jnp.float32
bf16 = jnp.bfloat16
EPS = 1e-06
LOG2E = math.log2(math.e)
FAR = -1e30
ROWS = 1024
AD = 64
MD = 128
QT = 256
N_SP, N_TP = 16, 8
VEXT = AD + 16
ZR = MD + 16


def dot(a, b):
    return jnp.dot(a, b, preferred_element_type=f32)


def pieces(x):
    hi = x.astype(bf16).astype(f32)
    rest = x - hi
    mid = rest.astype(bf16).astype(f32)
    low = (rest - mid).astype(bf16).astype(f32)
    return hi, mid, low


def halves(x):
    hi = x.astype(bf16)
    return hi, (x - hi.astype(f32)).astype(bf16)


def rows_of(values, height, width):
    at = lax.broadcasted_iota(jnp.int32, (height, width), 0)
    out = jnp.zeros((height, width), f32)
    for n, value in enumerate(values):
        out = jnp.where(at == n, value, out)
    return out


def project_kernel(tok, gain, wq, wk, wv, wmq, wmk, wmv, wmo, ing, shift,
                   q_o, kv_o, mq_o, mk_o, mv_o, mo_o, gate_o, w, sems):
    @pl.when(pl.program_id(0) == 0)
    def _():
        copies = []
        for n, (ref, at) in enumerate(
            ((wq, 0), (wk, 1), (wv, 2), (wmk, 3), (wmq, 4), (wmv, 5), (wmo, 6))
        ):
            copy = pltpu.make_async_copy(ref, w.at[:, at * 128 : at * 128 + 128], sems.at[n])
            copy.start()
            copies.append(copy)
        w[:, 896:1024] = jnp.zeros((2048, 128), bf16)
        w[:, 896:904] = ing[...]
        for copy in copies:
            copy.wait()

    x = tok[...].astype(f32)
    ms = jnp.mean(x * x, axis=-1, keepdims=True)
    n = (x * lax.rsqrt(ms + EPS) * gain[...]).astype(bf16)

    def unit(v):
        return (v * lax.rsqrt(jnp.mean(v * v, axis=0, keepdims=True) + EPS)).astype(bf16)

    def turned(p):
        return p.astype(bf16).astype(f32).T

    p = dot(n, w[:, 0:256])
    q, k = turned(p[:, :128]), turned(p[:, 128:])
    for h in range(2):
        q_o[h] = unit(q[h * AD : h * AD + AD])
        kv_o[h, 0:AD] = unit(k[h * AD : h * AD + AD])
    p = dot(n, w[:, 256:512])
    v = turned(p[:, :128]).astype(bf16)
    for h in range(2):
        kv_o[h, AD : 2 * AD] = v[h * AD : h * AD + AD]
    mk_o[...] = p[:, 128:].astype(bf16)
    p = dot(n, w[:, 512:768])
    mq_o[...] = turned(p[:, :128]).astype(bf16)
    mv_o[...] = turned(p[:, 128:]).astype(bf16)
    p = dot(n, w[:, 768:1024])
    mo_o[...] = turned(p[:, :128]).astype(bf16)
    gate_o[...] = p[:, 128:].T[0:8] + shift[...]


def project(tokens, gain, weights, ingate, shift):
    tile = 256
    hbm = pl.BlockSpec(memory_space=pl.ANY)

    def whole(shape):
        return pl.BlockSpec(shape, lambda i: (0,) * len(shape))

    lanes = lambda *lead: pl.BlockSpec((*lead, tile), lambda i: (0,) * len(lead) + (i,))
    return pl.pallas_call(
        project_kernel,
        grid=(ROWS // tile,),
        in_specs=[pl.BlockSpec((tile, 2048), lambda i: (i, 0)), whole((1, 2048))]
        + [hbm] * 7
        + [whole((2048, 8)), whole((8, 1))],
        out_specs=[
            lanes(2, AD), lanes(2, 2 * AD), lanes(MD),
            pl.BlockSpec((tile, MD), lambda i: (i, 0)),
            lanes(MD), lanes(MD), lanes(8),
        ],
        out_shape=[
            jax.ShapeDtypeStruct((2, AD, ROWS), bf16),
            jax.ShapeDtypeStruct((2, 2 * AD, ROWS), bf16),
            jax.ShapeDtypeStruct((MD, ROWS), bf16),
            jax.ShapeDtypeStruct((ROWS, MD), bf16),
            jax.ShapeDtypeStruct((MD, ROWS), bf16),
            jax.ShapeDtypeStruct((MD, ROWS), bf16),
            jax.ShapeDtypeStruct((8, ROWS), f32),
        ],
        scratch_shapes=[pltpu.VMEM((2048, 1024), bf16), pltpu.SemaphoreType.DMA((7,))],
        compiler_params=pltpu.CompilerParams(vmem_limit_bytes=48 * 2**20),
        cost_estimate=pl.CostEstimate(
            flops=2 * ROWS * 2048 * 1024, bytes_accessed=12 * 2**20, transcendentals=0
        ),
    )(tokens, gain, *weights, ingate, shift)


def shifted(x, by, fill):
    at = lax.broadcasted_iota(jnp.int32, x.shape, 1)
    return jnp.where(at >= by, pltpu.roll(x, by, 1), fill)


def scan_lanes(x, join, fill):
    by = 1
    while by < x.shape[1]:
        x = join(x, shifted(x, by, fill))
        by *= 2
    return x


def mix_kernel(scale_ref, q_in, kv_in, mq_in, mk_in, mv_in, mo_in, gate_in, fade_in, decay_in,
               cinit_in, ninit_in, again_in, mgain_in, wa_in, wm_in, out,
               wa, wm, kv, qb, decays, kaug, qaug, best, acc, ostage, att,
               zstage, zb, mstage, mb, mext, mnum,
               wsem, dsem, kv_s, kv_r, q_s, q_r, z_s, z_r, m_s, m_r, o_s, o_r, f_s, d_s, d_r):
    r = lax.axis_index("sp")
    t = lax.axis_index("tp")
    x, k = t // 2, t % 2
    g, a = r // 4, r % 4
    b = k
    hi = jnp.where(b == 0, 15 - a, 8 + a)
    lo = jnp.where(b == 0, a, 7 - a)
    both_to = 8 + a
    head = 4 * x + g

    barrier = pltpu.get_barrier_semaphore()
    me = r * N_TP + t

    def greet(n, _):
        other = (me + n) % (N_SP * N_TP)
        pl.semaphore_signal(
            barrier, inc=1, device_id=(other // N_TP, other % N_TP), device_id_type=MESH
        )
        return 0

    lax.fori_loop(1, N_SP * N_TP, greet, 0)

    w_copies = [
        pltpu.make_async_copy(wa_in, wa, wsem.at[0]),
        pltpu.make_async_copy(wm_in, wm, wsem.at[1]),
    ]
    for copy in w_copies:
        copy.start()
    own_decay = pltpu.make_async_copy(decay_in, decays.at[k], dsem)
    own_decay.start()

    gate = jnp.sum(
        jnp.where(lax.broadcasted_iota(jnp.int32, (8, ROWS), 0) == t, gate_in[...], 0.0),
        axis=0, keepdims=True,
    )
    fade = scan_lanes(jnp.broadcast_to(fade_in[...], (8, ROWS)), jnp.add, 0.0)
    level = jnp.broadcast_to(gate, (8, ROWS)) - fade
    crest8 = scan_lanes(level, jnp.maximum, FAR)
    crest = crest8[0:1]
    top = crest[:, ROWS - 1 : ROWS]
    total = fade[0:1, ROWS - 1 : ROWS]
    mext[0:MD] = mv_in[...]
    mext[MD:ZR] = jnp.ones((16, ROWS), bf16)
    weighted = mext[...].astype(f32) * jnp.exp(level[0:1] - top)
    w_hi, w_lo = halves(weighted)
    z = dot(w_hi, mk_in[...]) + dot(w_lo, mk_in[...])
    zstage[0:MD] = z[0:MD].astype(bf16)
    z_rest = (
        *pieces(z[MD : MD + 1]),
        *pieces(jnp.broadcast_to(total + top, (1, MD))),
        *pieces(jnp.broadcast_to(total, (1, MD))),
    )
    zstage[MD:ZR] = rows_of(z_rest, 16, MD).astype(bf16)

    pl.semaphore_wait(barrier, N_SP * N_TP - 1)

    def decay_copy():
        return pltpu.make_async_remote_copy(
            decay_in, decays.at[k], d_s, d_r, device_id=(r, 2 * x + 1 - k), device_id_type=MESH
        )

    decay_copy().start()

    def worker(chunk):
        quarter, low = chunk // 4, chunk % 4
        wa_ = jnp.where(quarter % 2 == 0, low, 3 - low)
        wb = jnp.where((quarter == 0) | (quarter == 3), 0, 1)
        slot = jnp.where(quarter >= 2, 0, 1)
        return wa_, wb, slot

    my_a, my_b, my_slot = worker(r)

    def q_copy(h):
        sp, tp = 4 * (2 * k + h) + my_a, 2 * x + my_b
        own = (sp == r) & (tp == t)
        return own, pltpu.make_async_remote_copy(
            q_in.at[h], qb.at[my_slot], q_s.at[h], q_r.at[my_slot],
            device_id=(sp, tp), device_id_type=MESH,
        )

    def kv_copy(h, to_a):
        sp = 4 * (2 * k + h) + to_a
        core = jnp.where(r <= 8 + to_a, r % 2, 0)
        tp = 2 * x + core
        own = (sp == r) & (tp == t)
        return (r <= 15 - to_a), own, pltpu.make_async_remote_copy(
            kv_in.at[h], kv.at[r, 0 : 2 * AD], kv_s.at[h * 4 + to_a], kv_r.at[r],
            device_id=(sp, tp), device_id_type=MESH,
        )

    for h in range(2):
        own, copy = q_copy(h)

        @pl.when(jnp.logical_not(own))
        def _():
            copy.start()

        @pl.when(own)
        def _():
            qb[my_slot] = q_in[h]

    def z_copy(to):
        return pltpu.make_async_remote_copy(
            zstage, zb.at[r], z_s.at[to], z_r.at[r], device_id=(to, t), device_id_type=MESH
        )

    def z_send(to, _):
        z_copy(to).start()
        return 0

    lax.fori_loop(r + 1, N_SP, z_send, 0)

    for h in range(2):
        for to_a in range(4):
            used, own, copy = kv_copy(h, to_a)

            @pl.when(used & jnp.logical_not(own))
            def _():
                copy.start()

            @pl.when(used & own)
            def _():
                kv[r, 0 : 2 * AD] = kv_in[h]

    levels = level.T
    for j in range(ROWS // QT):
        cols = slice(j * QT, j * QT + QT)
        n_keys = j * QT + QT
        raw = dot(mk_in[0:n_keys], mq_in[:, cols]) * MD**-0.5
        log = levels[0:n_keys, 0:1] - crest[:, cols]
        key_at = lax.broadcasted_iota(jnp.int32, (n_keys, QT), 0)
        query_at = lax.broadcasted_iota(jnp.int32, (n_keys, QT), 1) + j * QT
        seen = key_at <= query_at
        pair = jnp.where(seen, raw * jnp.exp(jnp.where(seen, log, 0.0)), 0.0)
        p_hi, p_lo = halves(pair)
        mnum[:, cols] = dot(mext[:, 0:n_keys], p_hi) + dot(mext[:, 0:n_keys], p_lo)

    own_decay.wait()
    decay_copy().wait_recv()
    factor = scale_ref[head] * (AD**-0.5 * LOG2E)

    def decay_of(chunk):
        slab = decays[g // 2, :, pl.ds(pl.multiple_of(chunk * ROWS, ROWS), ROWS)]
        return jnp.where(g % 2 == 0, slab[0:1], slab[1:2]) * LOG2E

    for slot in range(2):
        chunk = hi if slot == 0 else lo
        own = (chunk == r) & (g // 2 == k)

        @pl.when(jnp.logical_not(own))
        def _():
            pltpu.make_async_remote_copy(
                q_in.at[0], qb.at[slot], q_s.at[0], q_r.at[slot],
                device_id=(r, 2 * x + 1 - k), device_id_type=MESH,
            ).wait_recv()

        q_hi, q_mid, q_lo = pieces(qb[slot].astype(f32) * factor)
        d_hi, d_mid, d_lo = pieces(decay_of(chunk))
        qaug[slot, 0:64] = q_hi.astype(bf16)
        qaug[slot, 64:80] = rows_of((-1.0, -1.0, -1.0, d_hi, d_mid, d_lo), 16, ROWS).astype(bf16)
        qaug[slot, 80:128] = jnp.zeros((48, ROWS), bf16)
        qaug[slot, 128:192] = q_mid.astype(bf16)
        qaug[slot, 192:256] = q_lo.astype(bf16)
        best[slot] = jnp.full((8, ROWS), FAR, f32)
        acc[slot] = jnp.zeros((VEXT, ROWS), f32)

    def ones_row(chunk, _):
        kv[chunk, 2 * AD : 2 * AD + 16] = jnp.ones((16, ROWS), bf16)
        return 0

    lax.fori_loop(0, hi + 1, ones_row, 0)

    def forward_copy(chunk):
        return pltpu.make_async_remote_copy(
            kv.at[chunk, 0 : 2 * AD], kv.at[chunk, 0 : 2 * AD], f_s.at[chunk], kv_r.at[chunk],
            device_id=(r, 2 * x + 1 - k), device_id_type=MESH,
        )

    def forwards(chunk):
        return (chunk <= both_to) & (chunk % 2 == b)

    def arrive(chunk):
        own = (chunk == r) & (g // 2 == k) & (jnp.where(chunk <= both_to, chunk % 2, 0) == b)

        @pl.when(jnp.logical_not(own))
        def _():
            forward_copy(chunk).wait_recv()

        @pl.when(forwards(chunk))
        def _():
            forward_copy(chunk).start()

    def fold(slot, chunk, diag):
        def scores(i):
            n_keys = (i + 1) * QT if diag else ROWS
            s = dot(kaug[0:n_keys], qaug[slot, :, i * QT : i * QT + QT])
            if diag:
                key_at = lax.broadcasted_iota(jnp.int32, (n_keys, QT), 0)
                query_at = lax.broadcasted_iota(jnp.int32, (n_keys, QT), 1) + i * QT
                s = jnp.where(key_at <= query_at, s, FAR)
            return s

        def finish(i, s):
            cols = slice(i * QT, i * QT + QT)
            n_keys = s.shape[0]
            old = best[slot, 0:1, cols]
            new = jnp.maximum(old, jnp.max(s, axis=0, keepdims=True))
            weights = jnp.exp2(s - new).astype(bf16)
            got = dot(kv[chunk, AD : AD + VEXT, 0:n_keys], weights)
            acc[slot, :, cols] = acc[slot, :, cols] * jnp.exp2(old - new) + got
            best[slot, 0:1, cols] = new

        tiles = ROWS // QT
        s = scores(0)
        for i in range(tiles):
            later = scores(i + 1) if i + 1 < tiles else None
            finish(i, s)
            s = later

    arrive(0)

    def visit(chunk, _):
        @pl.when(chunk < hi)
        def _():
            arrive(chunk + 1)

        keys = kv[chunk, 0:AD]
        keys32 = keys.astype(f32)
        d_hi, d_mid, d_lo = pieces(decay_of(chunk))
        extra = rows_of((d_hi, d_mid, d_lo, 1.0, 1.0, 1.0), 64, ROWS)
        kaug[:, 0:128] = jnp.concatenate([keys32, extra], axis=0).T.astype(bf16)
        kaug[:, 128:256] = jnp.concatenate([keys32, keys32], axis=0).T.astype(bf16)

        def side(slot, _):
            mine = jnp.where(slot == 0, hi, lo)

            @pl.when(chunk < mine)
            def _():
                fold(slot, chunk, False)

            @pl.when(chunk == mine)
            def _():
                fold(slot, chunk, True)

            return 0

        lax.fori_loop(0, 2, side, 0)
        return 0

    lax.fori_loop(0, hi + 1, visit, 0)

    def o_copy(slot, p):
        chunk = hi if slot == 0 else lo
        own = (chunk == r) & (p == t)
        return own, pltpu.make_async_remote_copy(
            ostage.at[slot, p], att.at[head], o_s.at[slot, p], o_r.at[head],
            device_id=(chunk, p), device_id_type=MESH,
        )

    for slot in range(2):
        result = acc[slot, 0:AD] / acc[slot, AD : AD + 1]
        result = result.astype(bf16)
        for p in range(N_TP):
            ostage[slot, p] = result[:, p * 128 : p * 128 + 128]

        def o_send(p, _):
            own, copy = o_copy(slot, p)

            @pl.when(jnp.logical_not(own))
            def _():
                copy.start()

            @pl.when(own)
            def _():
                att[head] = ostage[slot, p]

            return 0

        lax.fori_loop(0, N_TP, o_send, 0)

    z0 = jnp.concatenate(
        [cinit_in[0].T, jnp.broadcast_to(ninit_in[...], (16, MD))], axis=0
    )

    def enter(n, carry):
        state, log = carry
        pltpu.make_async_remote_copy(
            zstage, zb.at[n], z_s.at[0], z_r.at[n], device_id=(0, t), device_id_type=MESH
        ).wait_recv()
        rest = zb[n, MD:ZR].astype(f32)
        norm = rest[0:1] + rest[1:2] + rest[2:3]
        stab = rest[3:4] + rest[4:5] + rest[5:6]
        faded = log + (rest[6:7] + rest[7:8] + rest[8:9])
        new = jnp.maximum(faded, stab)
        added = jnp.concatenate(
            [zb[n, 0:MD].astype(f32), jnp.broadcast_to(norm, (16, MD))], axis=0
        )
        return state * jnp.exp(faded - new) + added * jnp.exp(stab - new), new

    state, log = lax.fori_loop(0, r, enter, (z0, jnp.zeros((1, MD), f32)))
    log = log[:, 0:1]
    peak = jnp.maximum(crest, log)
    s_hi, s_lo = halves(state)
    carried = (dot(s_hi, mq_in[...]) + dot(s_lo, mq_in[...])) * MD**-0.5
    numer = mnum[...] * jnp.exp(crest - peak) + carried * jnp.exp(log - peak)
    floor = jnp.exp(-(fade[0:1] + peak))
    recalled = numer[0:MD] / jnp.maximum(jnp.abs(numer[MD : MD + 1]), floor)
    squares = jnp.sum(recalled * recalled, axis=0, keepdims=True)
    sq_hi, sq_mid, sq_lo = pieces(squares)
    gated = (recalled * jax.nn.sigmoid(mo_in[...].astype(f32))).astype(bf16)
    stats = rows_of((sq_hi, sq_mid, sq_lo), 16, ROWS).astype(bf16)
    for p in range(N_TP):
        mstage[p, 0:MD] = gated[:, p * 128 : p * 128 + 128]
        mstage[p, MD:ZR] = stats[:, p * 128 : p * 128 + 128]

    def m_copy(p):
        return pltpu.make_async_remote_copy(
            mstage.at[p], mb.at[t], m_s.at[p], m_r.at[t], device_id=(r, p), device_id_type=MESH
        )

    def m_send(p, _):
        @pl.when(p != t)
        def _():
            m_copy(p).start()

        @pl.when(p == t)
        def _():
            mb[t] = mstage[p]

        return 0

    lax.fori_loop(0, N_TP, m_send, 0)

    _, from_b, _ = worker(r)
    from_a, _, _ = worker(r)

    def o_wait(n, _):
        own = (n == head) & ((hi == r) | (lo == r))

        @pl.when(jnp.logical_not(own))
        def _():
            pltpu.make_async_remote_copy(
                ostage.at[0, 0], att.at[n], o_s.at[0, 0], o_r.at[n],
                device_id=(r, (t + 1) % N_TP), device_id_type=MESH,
            ).wait_recv()

        return 0

    def m_wait(n, _):
        @pl.when(n != t)
        def _():
            pltpu.make_async_remote_copy(
                mstage.at[0], mb.at[n], m_s.at[0], m_r.at[n],
                device_id=(r, (t + 1) % N_TP), device_id_type=MESH,
            ).wait_recv()

        return 0

    lax.fori_loop(0, N_TP, m_wait, 0)
    for copy in w_copies:
        copy.wait()

    m_all = jnp.concatenate([mb[n, 0:MD].astype(f32).T for n in range(N_TP)], axis=1)
    m_stats = sum(mb[n, MD:ZR].astype(f32) for n in range(N_TP)).T
    m_sq = m_stats[:, 0:1] + m_stats[:, 1:2] + m_stats[:, 2:3]
    m_mix = (m_all * lax.rsqrt(m_sq / 1024.0 + EPS) * mgain_in[...]).astype(bf16)

    lax.fori_loop(0, 16, o_wait, 0)
    a_all = jnp.concatenate(
        [
            jnp.concatenate([att[2 * n], att[2 * n + 1]], axis=0).astype(f32).T
            for n in range(8)
        ],
        axis=1,
    )
    a_sq = jnp.sum(a_all * a_all, axis=1, keepdims=True)
    a_mix = (a_all * lax.rsqrt(a_sq / 1024.0 + EPS) * again_in[...]).astype(bf16)
    for n in range(4):
        cols = slice(n * 512, n * 512 + 512)
        out[:, cols] = (dot(m_mix, wm[:, cols]) + dot(a_mix, wa[:, cols])).astype(bf16)

    decay_copy().wait_send()
    for h in range(2):
        own, copy = q_copy(h)

        @pl.when(jnp.logical_not(own))
        def _():
            copy.wait_send()

        for to_a in range(4):
            used, own, copy = kv_copy(h, to_a)

            @pl.when(used & jnp.logical_not(own))
            def _():
                copy.wait_send()

    def z_done(to, _):
        z_copy(to).wait_send()
        return 0

    lax.fori_loop(r + 1, N_SP, z_done, 0)

    def f_done(chunk, _):
        @pl.when(forwards(chunk))
        def _():
            forward_copy(chunk).wait_send()

        return 0

    lax.fori_loop(0, hi + 1, f_done, 0)

    def p_done(p, _):
        for slot in range(2):
            own, copy = o_copy(slot, p)

            @pl.when(jnp.logical_not(own))
            def _():
                copy.wait_send()

        @pl.when(p != t)
        def _():
            m_copy(p).wait_send()

        return 0

    lax.fori_loop(0, N_TP, p_done, 0)


def mix(*arrays):
    vmem = pl.BlockSpec(memory_space=pltpu.VMEM)
    hbm = pl.BlockSpec(memory_space=pl.ANY)
    dma = pltpu.SemaphoreType.DMA
    return pl.pallas_call(
        mix_kernel,
        out_shape=jax.ShapeDtypeStruct((128, 2048), bf16),
        in_specs=[pl.BlockSpec(memory_space=pltpu.SMEM)] + [vmem] * 8 + [hbm]
        + [vmem] * 4 + [hbm] * 2,
        out_specs=vmem,
        scratch_shapes=[
            pltpu.VMEM((1024, 2048), bf16),
            pltpu.VMEM((1024, 2048), bf16),
            pltpu.VMEM((N_SP, 2 * AD + 16, ROWS), bf16),
            pltpu.VMEM((2, AD, ROWS), bf16),
            pltpu.VMEM((2, 2, N_SP * ROWS), f32),
            pltpu.VMEM((ROWS, 256), bf16),
            pltpu.VMEM((2, 256, ROWS), bf16),
            pltpu.VMEM((2, 8, ROWS), f32),
            pltpu.VMEM((2, VEXT, ROWS), f32),
            pltpu.VMEM((2, N_TP, AD, 128), bf16),
            pltpu.VMEM((16, AD, 128), bf16),
            pltpu.VMEM((ZR, MD), bf16),
            pltpu.VMEM((N_SP, ZR, MD), bf16),
            pltpu.VMEM((N_TP, ZR, 128), bf16),
            pltpu.VMEM((N_TP, ZR, 128), bf16),
            pltpu.VMEM((ZR, ROWS), bf16),
            pltpu.VMEM((ZR, ROWS), f32),
            dma((2,)), dma,
            dma((8,)), dma((N_SP,)),
            dma((2,)), dma((2,)),
            dma((N_SP,)), dma((N_SP,)),
            dma((N_TP,)), dma((N_TP,)),
            dma((2, N_TP)), dma((16,)),
            dma((N_SP,)), dma, dma,
        ],
        compiler_params=pltpu.CompilerParams(
            collective_id=0, has_side_effects=True, vmem_limit_bytes=60 * 2**20
        ),
        cost_estimate=pl.CostEstimate(
            flops=60 * 10**9, bytes_accessed=12 * 2**20, transcendentals=0
        ),
    )(*arrays)


def on_device(tokens, norm_gain, attn_query, attn_key, attn_value, score_scale, attention_decay,
              mem_query, mem_key, mem_value, mem_ingate, input_shift, memory_decay, mem_outgate,
              init_memory, init_normalizer, attn_gain, mem_gain, attn_out, mem_out):
    q, kv, mq, mk, mv, mo, gate = project(
        tokens, norm_gain.reshape(1, 2048),
        (attn_query, attn_key, attn_value, mem_query, mem_key, mem_value, mem_outgate),
        mem_ingate, input_shift.reshape(8, 1),
    )
    return mix(
        score_scale, q, kv, mq, mk, mv, mo, gate, memory_decay, attention_decay,
        init_memory, init_normalizer, attn_gain.reshape(1, 1024), mem_gain.reshape(1, 1024),
        attn_out, mem_out,
    )


def solution(mesh):
    tp = P(None, "tp")
    placed = (
        P("sp", None), P(), tp, tp, tp, P(), P("tp", None), tp, tp, tp, P(), P(),
        P("tp", "sp"), tp, P("tp", None, None), P("tp", None), P(), P(), P(), P(),
    )
    return jax.shard_map(
        on_device, mesh=mesh, in_specs=placed, out_specs=P(("sp", "tp"), None), check_vma=False
    )
```

time: 381 us -> 140 us (0.37)
  the two profiles are of different devices: /device:TPU:120 before, /device:TPU:1 now
where the time goes in v1:
time: 140 us; the launch traced here: 139 us
  Pallas kernels  122 us (87%)
  local copies, waits for them, and re-layouts  16.6 us (12%)
    pallas_call x1, Pallas kernels, mix(): pl.pallas_call(mix_kernel, out_shape=jax.ShapeDtypeStruct((128, 2048), bf...  113 us
    unnamed x32, local copies, waits for them, and re-layouts  15.8 us
    pallas_call x1, Pallas kernels, project(): pl.pallas_call(project_kernel, grid=(ROWS // tile,), in_specs=[pl.BlockSp...  9.28 us

profile of v1, /device:TPU:1, one launch (start us, length us, event | category | flops | bytes accessed | tf_op | source)
XLA Modules:
  0.0 139.0 jit_solution(990237856548867426)
XLA Ops:
  0.0 0.7 copy.22.shift
  0.7 1.0 copy.21.ing
  1.8 0.0 copy-start
  1.8 1.0 copy-done
  2.8 0.0 copy-start.1
  2.8 1.0 copy-done.1
  3.9 0.0 copy-start.2
  3.9 1.0 copy-done.2
  4.9 0.0 copy-start.3
  4.9 1.0 copy-done.3
  6.0 0.0 copy-start.4
  6.0 1.0 copy-done.4
  7.0 1.0 copy-done.5
  8.0 0.0 copy-start.6
  8.0 1.0 copy-done.6
  9.1 0.0 copy-start.7
  9.1 0.7 copy-done.7
  9.8 9.3 %shard_map.190 = (bf16[2,64,1024]{2,1,0:T(8,128)(2,1)S(1)}, bf16[2,128,1024]{2,1,0:T(8,128)(2,1)S(1)}, bf16[128,1024]{1,0:T(8,128)(2,1)S(1)}, bf16[1024,128]{1,0...) custom-call(bf16[1024,2048]{1,0:T(8,128)(2,1)} %tok.1, ...), custom_call_target="tpu_custom_call" | custom-call | flops 4294967296 | bytes 12582912 | tf_op jit(solution)/shard_map/pallas_call | solution.py:103
  19.1 0.0 copy-start.8
  19.1 0.8 copy-done.8
  19.9 0.0 copy-start.9
  19.9 0.7 copy-done.9
  20.6 0.0 copy-start.10
  20.6 0.7 copy-done.10
  21.3 0.0 copy-start.11
  21.3 0.7 copy-done.11
  22.0 0.0 copy-start.12
  22.0 0.7 copy-done.12
  22.7 0.7 copy-done.13
  23.4 0.6 copy-done.14
  24.0 113.1 %shard_map.191 = bf16[128,2048]{1,0:T(8,128)(2,1)} custom-call(f32[16]{0:T(128)} %scale_ref.1, bf16[2,64,1024]{2,1,0:T(8,128)(2,1)} %copy-done.9, bf16[2,128,1024]{2,1,0:T(8,128)(2,1)} %copy-done.8, bf16[128,1024]{1,0:T(8,128)(2,1)} %copy-done.10, bf16[1024,128]{1,0:T(8,128)(2,1)} %copy-done.11, bf16[128,1024]{1,0:T(8,128)(2,1)} %copy-done.12, ...), custom_call_target="tpu_custom_call" | custom-call | flops 60000002048 | bytes 12582912 | tf_op jit(solution)/shard_map/pallas_call | solution.py:581
  137.1 1.9 %copy.24 = bf16[128,2048]{1,0:T(8,128)(2,1)} copy(bf16[128,2048]{1,0:T(8,128)(2,1)} %shard_map.191) | data formatting | bytes 1048576
  (3 shorter events, 0.0 us)
Async XLA Ops:
  1.8 1.0 copy-start
  2.8 1.0 copy-start.1
  3.9 1.0 copy-start.2
  4.9 1.0 copy-start.3
  6.0 1.0 copy-start.4
  7.0 1.0 copy-start.5
  8.0 1.0 copy-start.6
  9.1 0.7 copy-start.7
  19.1 0.8 copy-start.8
  19.9 0.7 copy-start.9
  20.6 0.7 copy-start.10
  21.3 0.7 copy-start.11
  22.0 0.7 copy-start.12
  22.7 0.7 copy-start.13
  23.4 0.6 copy-start.14

commit v2 on v1

--- a/solution.py
+++ b/solution.py
@@ -48,86 +48,6 @@
     return out
 
 
-def project_kernel(tok, gain, wq, wk, wv, wmq, wmk, wmv, wmo, ing, shift,
-                   q_o, kv_o, mq_o, mk_o, mv_o, mo_o, gate_o, w, sems):
-    @pl.when(pl.program_id(0) == 0)
-    def _():
-        copies = []
-        for n, (ref, at) in enumerate(
-            ((wq, 0), (wk, 1), (wv, 2), (wmk, 3), (wmq, 4), (wmv, 5), (wmo, 6))
-        ):
-            copy = pltpu.make_async_copy(ref, w.at[:, at * 128 : at * 128 + 128], sems.at[n])
-            copy.start()
-            copies.append(copy)
-        w[:, 896:1024] = jnp.zeros((2048, 128), bf16)
-        w[:, 896:904] = ing[...]
-        for copy in copies:
-            copy.wait()
-
-    x = tok[...].astype(f32)
-    ms = jnp.mean(x * x, axis=-1, keepdims=True)
-    n = (x * lax.rsqrt(ms + EPS) * gain[...]).astype(bf16)
-
-    def unit(v):
-        return (v * lax.rsqrt(jnp.mean(v * v, axis=0, keepdims=True) + EPS)).astype(bf16)
-
-    def turned(p):
-        return p.astype(bf16).astype(f32).T
-
-    p = dot(n, w[:, 0:256])
-    q, k = turned(p[:, :128]), turned(p[:, 128:])
-    for h in range(2):
-        q_o[h] = unit(q[h * AD : h * AD + AD])
-        kv_o[h, 0:AD] = unit(k[h * AD : h * AD + AD])
-    p = dot(n, w[:, 256:512])
-    v = turned(p[:, :128]).astype(bf16)
-    for h in range(2):
-        kv_o[h, AD : 2 * AD] = v[h * AD : h * AD + AD]
-    mk_o[...] = p[:, 128:].astype(bf16)
-    p = dot(n, w[:, 512:768])
-    mq_o[...] = turned(p[:, :128]).astype(bf16)
-    mv_o[...] = turned(p[:, 128:]).astype(bf16)
-    p = dot(n, w[:, 768:1024])
-    mo_o[...] = turned(p[:, :128]).astype(bf16)
-    gate_o[...] = p[:, 128:].T[0:8] + shift[...]
-
-
-def project(tokens, gain, weights, ingate, shift):
-    tile = 256
-    hbm = pl.BlockSpec(memory_space=pl.ANY)
-
-    def whole(shape):
-        return pl.BlockSpec(shape, lambda i: (0,) * len(shape))
-
-    lanes = lambda *lead: pl.BlockSpec((*lead, tile), lambda i: (0,) * len(lead) + (i,))
-    return pl.pallas_call(
-        project_kernel,
-        grid=(ROWS // tile,),
-        in_specs=[pl.BlockSpec((tile, 2048), lambda i: (i, 0)), whole((1, 2048))]
-        + [hbm] * 7
-        + [whole((2048, 8)), whole((8, 1))],
-        out_specs=[
-            lanes(2, AD), lanes(2, 2 * AD), lanes(MD),
-            pl.BlockSpec((tile, MD), lambda i: (i, 0)),
-            lanes(MD), lanes(MD), lanes(8),
-        ],
-        out_shape=[
-            jax.ShapeDtypeStruct((2, AD, ROWS), bf16),
-            jax.ShapeDtypeStruct((2, 2 * AD, ROWS), bf16),
-            jax.ShapeDtypeStruct((MD, ROWS), bf16),
-            jax.ShapeDtypeStruct((ROWS, MD), bf16),
-            jax.ShapeDtypeStruct((MD, ROWS), bf16),
-            jax.ShapeDtypeStruct((MD, ROWS), bf16),
-            jax.ShapeDtypeStruct((8, ROWS), f32),
-        ],
-        scratch_shapes=[pltpu.VMEM((2048, 1024), bf16), pltpu.SemaphoreType.DMA((7,))],
-        compiler_params=pltpu.CompilerParams(vmem_limit_bytes=48 * 2**20),
-        cost_estimate=pl.CostEstimate(
-            flops=2 * ROWS * 2048 * 1024, bytes_accessed=12 * 2**20, transcendentals=0
-        ),
-    )(tokens, gain, *weights, ingate, shift)
-
-
 def shifted(x, by, fill):
     at = lax.broadcasted_iota(jnp.int32, x.shape, 1)
     return jnp.where(at >= by, pltpu.roll(x, by, 1), fill)
@@ -141,20 +61,59 @@
     return x
 
 
-def mix_kernel(scale_ref, q_in, kv_in, mq_in, mk_in, mv_in, mo_in, gate_in, fade_in, decay_in,
-               cinit_in, ninit_in, again_in, mgain_in, wa_in, wm_in, out,
+def mix_kernel(scale_ref, shift_ref, tok_in, wq_in, wk_in, wv_in, wmq_in, wmk_in, wmv_in, wmo_in, ing_in,
+               ngain_in, fade_hbm, decay_in, cinit_hbm, ninit_hbm, again_hbm, mgain_hbm, wa_in, wm_in,
+               out, tok, w, ing, ngain, fade_in, cinit_in, ninit_in, again_in, mgain_in,
+               qs, kvs, mq_in, mk_in, mo_in, fade_s, crest_s, levels,
                wa, wm, kv, qb, decays, kaug, qaug, best, acc, ostage, att,
                zstage, zb, mstage, mb, mext, mnum,
-               wsem, dsem, kv_s, kv_r, q_s, q_r, z_s, z_r, m_s, m_r, o_s, o_r, f_s, d_s, d_r):
+               isem, wsem, kv_s, kv_r, q_s, q_r, z_s, z_r, m_s, m_r, o_s, o_r, p_s, f_s, d_s, d_r):
     r = lax.axis_index("sp")
     t = lax.axis_index("tp")
     x, k = t // 2, t % 2
-    g, a = r // 4, r % 4
+    rz, ry = r // 4, r % 4
+    g = 2 * (rz // 2) + ry // 2
+    a = 2 * (rz % 2) + ry % 2
     b = k
     hi = jnp.where(b == 0, 15 - a, 8 + a)
     lo = jnp.where(b == 0, a, 7 - a)
-    both_to = 8 + a
     head = 4 * x + g
+
+    def chip_of(block, member):
+        z = 2 * (block // 2) + member // 2
+        y = 2 * (block % 2) + member % 2
+        return 4 * z + y
+
+    def flip(v):
+        return v + 1 - 2 * (v % 2)
+
+    def core_for(chunk):
+        return (chunk % 4) // 2
+
+    loads = []
+
+    def load(src, dst):
+        copy = pltpu.make_async_copy(src, dst, isem.at[len(loads)])
+        copy.start()
+        loads.append(copy)
+        return copy
+
+    small = [
+        load(ngain_in, ngain), load(ing_in, ing), load(fade_hbm, fade_in), load(cinit_hbm, cinit_in),
+        load(ninit_hbm, ninit_in), load(again_hbm, again_in), load(mgain_hbm, mgain_in),
+    ]
+    tok_loads = []
+    first = []
+    rest = []
+    for i in range(4):
+        rows = slice(i * 256, i * 256 + 256)
+        tok_loads.append(load(tok_in.at[rows], tok.at[rows]))
+        if i == 0:
+            for n, ref in ((0, wq_in), (1, wk_in), (2, wv_in), (3, wmk_in)):
+                first.append(load(ref, w.at[:, n * 128 : n * 128 + 128]))
+    for n, ref in ((4, wmq_in), (5, wmv_in), (6, wmo_in)):
+        rest.append(load(ref, w.at[:, n * 128 : n * 128 + 128]))
+    own_decay = load(decay_in, decays.at[k])
 
     barrier = pltpu.get_barrier_semaphore()
     me = r * N_TP + t
@@ -168,26 +127,121 @@
 
     lax.fori_loop(1, N_SP * N_TP, greet, 0)
 
-    w_copies = [
-        pltpu.make_async_copy(wa_in, wa, wsem.at[0]),
-        pltpu.make_async_copy(wm_in, wm, wsem.at[1]),
-    ]
-    for copy in w_copies:
-        copy.start()
-    own_decay = pltpu.make_async_copy(decay_in, decays.at[k], dsem)
-    own_decay.start()
-
+    for copy in small:
+        copy.wait()
+    for copy in first:
+        copy.wait()
+
+    def unit(v):
+        return (v * lax.rsqrt(jnp.mean(v * v, axis=0, keepdims=True) + EPS)).astype(bf16)
+
+    def turned(p):
+        return p.astype(bf16).astype(f32).T
+
+    for i in range(4):
+        rows = slice(i * 256, i * 256 + 256)
+        tok_loads[i].wait()
+        v = tok[rows].astype(f32)
+        ms = jnp.mean(v * v, axis=-1, keepdims=True)
+        n = (v * lax.rsqrt(ms + EPS) * ngain[...]).astype(bf16)
+        tok[rows] = n
+        p = dot(n, w[:, 0:256])
+        pq, pk = turned(p[:, :128]), turned(p[:, 128:])
+        for h in range(2):
+            qs[h, :, rows] = unit(pq[h * AD : h * AD + AD])
+            kvs[h, 0:AD, rows] = unit(pk[h * AD : h * AD + AD])
+        p = dot(n, w[:, 256:512])
+        pv = turned(p[:, :128]).astype(bf16)
+        for h in range(2):
+            kvs[h, AD : 2 * AD, rows] = pv[h * AD : h * AD + AD]
+        mk_in[rows] = p[:, 128:].astype(bf16)
+
+    pl.semaphore_wait(barrier, N_SP * N_TP - 1)
+
+    def worker(chunk):
+        quarter, low = chunk // 4, chunk % 4
+        wa_ = jnp.where(quarter % 2 == 0, low, 3 - low)
+        wb = jnp.where((quarter == 0) | (quarter == 3), 0, 1)
+        slot = jnp.where(quarter >= 2, 0, 1)
+        return wa_, wb, slot
+
+    my_a, my_b, my_slot = worker(r)
+
+    def q_copy(h):
+        sp, tp = chip_of(2 * k + h, my_a), 2 * x + my_b
+        own = (sp == r) & (tp == t)
+        return own, pltpu.make_async_remote_copy(
+            qs.at[h], qb.at[my_slot], q_s.at[h], q_r.at[my_slot],
+            device_id=(sp, tp), device_id_type=MESH,
+        )
+
+    def kv_copy(h):
+        block = 2 * k + h
+        z = jnp.where(rz // 2 == block // 2, rz, 3 - rz)
+        y = jnp.where(ry // 2 == block % 2, ry, 3 - ry)
+        sp, tp = 4 * z + y, 2 * x + core_for(r)
+        own = (sp == r) & (tp == t)
+        return own, pltpu.make_async_remote_copy(
+            kvs.at[h], kv.at[r, 0 : 2 * AD], kv_s.at[h], kv_r.at[r],
+            device_id=(sp, tp), device_id_type=MESH,
+        )
+
+    for h in range(2):
+        own, copy = kv_copy(h)
+
+        @pl.when(jnp.logical_not(own))
+        def _():
+            copy.start()
+
+        @pl.when(own)
+        def _():
+            kv[r, 0 : 2 * AD] = kvs[h]
+
+    def decay_copy():
+        return pltpu.make_async_remote_copy(
+            decay_in, decays.at[k], d_s, d_r, device_id=(r, 2 * x + 1 - k), device_id_type=MESH
+        )
+
+    decay_copy().start()
+    for h in range(2):
+        own, copy = q_copy(h)
+
+        @pl.when(jnp.logical_not(own))
+        def _():
+            copy.start()
+
+        @pl.when(own)
+        def _():
+            qb[my_slot] = qs[h]
+
+    w[:, 896:1024] = jnp.zeros((2048, 128), bf16)
+    w[:, 896:904] = ing[...].astype(f32).T.astype(bf16)
+    for copy in rest:
+        copy.wait()
+    gates = []
+    for i in range(4):
+        rows = slice(i * 256, i * 256 + 256)
+        p = dot(tok[rows], w[:, 512:768])
+        mq_in[:, rows] = turned(p[:, :128]).astype(bf16)
+        mext[0:MD, rows] = turned(p[:, 128:]).astype(bf16)
+        p = dot(tok[rows], w[:, 768:1024])
+        mo_in[:, rows] = turned(p[:, :128]).astype(bf16)
+        gates.append(p[:, 128:].T[0:8])
+
+    gate8 = jnp.concatenate(gates, axis=1)
     gate = jnp.sum(
-        jnp.where(lax.broadcasted_iota(jnp.int32, (8, ROWS), 0) == t, gate_in[...], 0.0),
+        jnp.where(lax.broadcasted_iota(jnp.int32, (8, ROWS), 0) == t, gate8, 0.0),
         axis=0, keepdims=True,
-    )
+    ) + shift_ref[t]
     fade = scan_lanes(jnp.broadcast_to(fade_in[...], (8, ROWS)), jnp.add, 0.0)
     level = jnp.broadcast_to(gate, (8, ROWS)) - fade
     crest8 = scan_lanes(level, jnp.maximum, FAR)
+    fade_s[...] = fade
+    crest_s[...] = crest8
+    levels[...] = level.T
     crest = crest8[0:1]
     top = crest[:, ROWS - 1 : ROWS]
     total = fade[0:1, ROWS - 1 : ROWS]
-    mext[0:MD] = mv_in[...]
     mext[MD:ZR] = jnp.ones((16, ROWS), bf16)
     weighted = mext[...].astype(f32) * jnp.exp(level[0:1] - top)
     w_hi, w_lo = halves(weighted)
@@ -200,53 +254,6 @@
     )
     zstage[MD:ZR] = rows_of(z_rest, 16, MD).astype(bf16)
 
-    pl.semaphore_wait(barrier, N_SP * N_TP - 1)
-
-    def decay_copy():
-        return pltpu.make_async_remote_copy(
-            decay_in, decays.at[k], d_s, d_r, device_id=(r, 2 * x + 1 - k), device_id_type=MESH
-        )
-
-    decay_copy().start()
-
-    def worker(chunk):
-        quarter, low = chunk // 4, chunk % 4
-        wa_ = jnp.where(quarter % 2 == 0, low, 3 - low)
-        wb = jnp.where((quarter == 0) | (quarter == 3), 0, 1)
-        slot = jnp.where(quarter >= 2, 0, 1)
-        return wa_, wb, slot
-
-    my_a, my_b, my_slot = worker(r)
-
-    def q_copy(h):
-        sp, tp = 4 * (2 * k + h) + my_a, 2 * x + my_b
-        own = (sp == r) & (tp == t)
-        return own, pltpu.make_async_remote_copy(
-            q_in.at[h], qb.at[my_slot], q_s.at[h], q_r.at[my_slot],
-            device_id=(sp, tp), device_id_type=MESH,
-        )
-
-    def kv_copy(h, to_a):
-        sp = 4 * (2 * k + h) + to_a
-        core = jnp.where(r <= 8 + to_a, r % 2, 0)
-        tp = 2 * x + core
-        own = (sp == r) & (tp == t)
-        return (r <= 15 - to_a), own, pltpu.make_async_remote_copy(
-            kv_in.at[h], kv.at[r, 0 : 2 * AD], kv_s.at[h * 4 + to_a], kv_r.at[r],
-            device_id=(sp, tp), device_id_type=MESH,
-        )
-
-    for h in range(2):
-        own, copy = q_copy(h)
-
-        @pl.when(jnp.logical_not(own))
-        def _():
-            copy.start()
-
-        @pl.when(own)
-        def _():
-            qb[my_slot] = q_in[h]
-
     def z_copy(to):
         return pltpu.make_async_remote_copy(
             zstage, zb.at[r], z_s.at[to], z_r.at[r], device_id=(to, t), device_id_type=MESH
@@ -256,21 +263,60 @@
         z_copy(to).start()
         return 0
 
+    def chunk_at(n):
+        p, m = n // 4, n % 4
+        pz = jnp.where(p // 2 == 1, flip(rz), rz)
+        py = jnp.where(p % 2 == 1, flip(ry), ry)
+        cz = jnp.where(m // 2 == 1, 3 - pz, pz)
+        cy = jnp.where(m % 2 == 1, 3 - py, py)
+        return 4 * cz + cy
+
+    def sibling_uses(chunk):
+        return jnp.where(b == 0, chunk <= 8 + a, chunk <= 15 - a)
+
+    def forward_copy(chunk):
+        return pltpu.make_async_remote_copy(
+            kv.at[chunk, 0 : 2 * AD], kv.at[chunk, 0 : 2 * AD], f_s.at[chunk], kv_r.at[chunk],
+            device_id=(r, 2 * x + 1 - k), device_id_type=MESH,
+        )
+
+    def peer_copy(chunk, n, p):
+        member = jnp.where(p // 2 == 1, 2 - 2 * (a // 2), 2 * (a // 2)) + jnp.where(
+            p % 2 == 1, 1 - a % 2, a % 2
+        )
+        return (chunk <= 15 - member), pltpu.make_async_remote_copy(
+            kv.at[chunk, 0 : 2 * AD], kv.at[chunk, 0 : 2 * AD], p_s.at[n % 4, p - 1], kv_r.at[chunk],
+            device_id=(chip_of(g, member), t), device_id_type=MESH,
+        )
+
+    def arrive(n, entry):
+        chunk = chunk_at(n)
+        mine = core_for(chunk) == b
+        used = jnp.where(mine, True, jnp.where(b == 0, chunk <= 15 - a, chunk <= 8 + a))
+        reaches = True if entry else chunk <= 15 - a
+        own = (chunk == r) & (g // 2 == k) & mine
+
+        @pl.when(reaches & used & jnp.logical_not(own))
+        def _():
+            forward_copy(chunk).wait_recv()
+
+        @pl.when(reaches & mine)
+        def _():
+            for p in (1, 2, 3) if entry else ():
+                wanted, copy = peer_copy(chunk, n, p)
+
+                @pl.when(wanted)
+                def _():
+                    copy.start()
+
+            @pl.when(sibling_uses(chunk))
+            def _():
+                forward_copy(chunk).start()
+
+    for n in range(4):
+        arrive(n, True)
     lax.fori_loop(r + 1, N_SP, z_send, 0)
 
-    for h in range(2):
-        for to_a in range(4):
-            used, own, copy = kv_copy(h, to_a)
-
-            @pl.when(used & jnp.logical_not(own))
-            def _():
-                copy.start()
-
-            @pl.when(used & own)
-            def _():
-                kv[r, 0 : 2 * AD] = kv_in[h]
-
-    levels = level.T
     for j in range(ROWS // QT):
         cols = slice(j * QT, j * QT + QT)
         n_keys = j * QT + QT
@@ -283,6 +329,12 @@
         p_hi, p_lo = halves(pair)
         mnum[:, cols] = dot(mext[:, 0:n_keys], p_hi) + dot(mext[:, 0:n_keys], p_lo)
 
+    w_copies = []
+    for n in range(8):
+        rows = slice(n % 4 * 256, n % 4 * 256 + 256)
+        src, dst = ((wa_in, wa), (wm_in, wm))[n // 4]
+        w_copies.append(pltpu.make_async_copy(src.at[rows], dst.at[rows], wsem.at[n]))
+        w_copies[-1].start()
     own_decay.wait()
     decay_copy().wait_recv()
     factor = scale_ref[head] * (AD**-0.5 * LOG2E)
@@ -298,7 +350,7 @@
         @pl.when(jnp.logical_not(own))
         def _():
             pltpu.make_async_remote_copy(
-                q_in.at[0], qb.at[slot], q_s.at[0], q_r.at[slot],
+                qs.at[0], qb.at[slot], q_s.at[0], q_r.at[slot],
                 device_id=(r, 2 * x + 1 - k), device_id_type=MESH,
             ).wait_recv()
 
@@ -316,27 +368,7 @@
         kv[chunk, 2 * AD : 2 * AD + 16] = jnp.ones((16, ROWS), bf16)
         return 0
 
-    lax.fori_loop(0, hi + 1, ones_row, 0)
-
-    def forward_copy(chunk):
-        return pltpu.make_async_remote_copy(
-            kv.at[chunk, 0 : 2 * AD], kv.at[chunk, 0 : 2 * AD], f_s.at[chunk], kv_r.at[chunk],
-            device_id=(r, 2 * x + 1 - k), device_id_type=MESH,
-        )
-
-    def forwards(chunk):
-        return (chunk <= both_to) & (chunk % 2 == b)
-
-    def arrive(chunk):
-        own = (chunk == r) & (g // 2 == k) & (jnp.where(chunk <= both_to, chunk % 2, 0) == b)
-
-        @pl.when(jnp.logical_not(own))
-        def _():
-            forward_copy(chunk).wait_recv()
-
-        @pl.when(forwards(chunk))
-        def _():
-            forward_copy(chunk).start()
+    lax.fori_loop(0, N_SP, ones_row, 0)
 
     def fold(slot, chunk, diag):
         def scores(i):
@@ -365,13 +397,20 @@
             finish(i, s)
             s = later
 
-    arrive(0)
-
-    def visit(chunk, _):
-        @pl.when(chunk < hi)
-        def _():
-            arrive(chunk + 1)
-
+    def visit(n, _):
+        @pl.when((n >= 3) & (n < 15))
+        def _():
+            arrive(n + 1, False)
+
+        chunk = chunk_at(n)
+
+        @pl.when(chunk <= hi)
+        def _():
+            take(chunk)
+
+        return 0
+
+    def take(chunk):
         keys = kv[chunk, 0:AD]
         keys32 = keys.astype(f32)
         d_hi, d_mid, d_lo = pieces(decay_of(chunk))
@@ -393,9 +432,8 @@
             return 0
 
         lax.fori_loop(0, 2, side, 0)
-        return 0
-
-    lax.fori_loop(0, hi + 1, visit, 0)
+
+    lax.fori_loop(0, 16, visit, 0)
 
     def o_copy(slot, p):
         chunk = hi if slot == 0 else lo
@@ -446,12 +484,13 @@
         return state * jnp.exp(faded - new) + added * jnp.exp(stab - new), new
 
     state, log = lax.fori_loop(0, r, enter, (z0, jnp.zeros((1, MD), f32)))
+    crest = crest_s[0:1]
     log = log[:, 0:1]
     peak = jnp.maximum(crest, log)
     s_hi, s_lo = halves(state)
     carried = (dot(s_hi, mq_in[...]) + dot(s_lo, mq_in[...])) * MD**-0.5
     numer = mnum[...] * jnp.exp(crest - peak) + carried * jnp.exp(log - peak)
-    floor = jnp.exp(-(fade[0:1] + peak))
+    floor = jnp.exp(-(fade_s[0:1] + peak))
     recalled = numer[0:MD] / jnp.maximum(jnp.abs(numer[MD : MD + 1]), floor)
     squares = jnp.sum(recalled * recalled, axis=0, keepdims=True)
     sq_hi, sq_mid, sq_lo = pieces(squares)
@@ -478,9 +517,6 @@
         return 0
 
     lax.fori_loop(0, N_TP, m_send, 0)
-
-    _, from_b, _ = worker(r)
-    from_a, _, _ = worker(r)
 
     def o_wait(n, _):
         own = (n == head) & ((hi == r) | (lo == r))
@@ -529,16 +565,9 @@
 
     decay_copy().wait_send()
     for h in range(2):
-        own, copy = q_copy(h)
-
-        @pl.when(jnp.logical_not(own))
-        def _():
-            copy.wait_send()
-
-        for to_a in range(4):
-            used, own, copy = kv_copy(h, to_a)
-
-            @pl.when(used & jnp.logical_not(own))
+        for own, copy in (q_copy(h), kv_copy(h)):
+
+            @pl.when(jnp.logical_not(own))
             def _():
                 copy.wait_send()
 
@@ -548,14 +577,29 @@
 
     lax.fori_loop(r + 1, N_SP, z_done, 0)
 
-    def f_done(chunk, _):
-        @pl.when(forwards(chunk))
-        def _():
-            forward_copy(chunk).wait_send()
-
-        return 0
-
-    lax.fori_loop(0, hi + 1, f_done, 0)
+    def f_done(n, _):
+        chunk = chunk_at(n)
+        mine = core_for(chunk) == b
+        reaches = jnp.where(n < 4, True, chunk <= 15 - a)
+
+        @pl.when(reaches & mine)
+        def _():
+            @pl.when(n < 4)
+            def _():
+                for p in (1, 2, 3):
+                    wanted, copy = peer_copy(chunk, n, p)
+
+                    @pl.when(wanted)
+                    def _():
+                        copy.wait_send()
+
+            @pl.when(sibling_uses(chunk))
+            def _():
+                forward_copy(chunk).wait_send()
+
+        return 0
+
+    lax.fori_loop(0, N_SP, f_done, 0)
 
     def p_done(p, _):
         for slot in range(2):
@@ -575,16 +619,32 @@
 
 
 def mix(*arrays):
-    vmem = pl.BlockSpec(memory_space=pltpu.VMEM)
-    hbm = pl.BlockSpec(memory_space=pl.ANY)
+    smem = pl.BlockSpec(memory_space=pltpu.SMEM)
+    hbm = pl.BlockSpec(memory_space=pltpu.HBM)
     dma = pltpu.SemaphoreType.DMA
     return pl.pallas_call(
         mix_kernel,
         out_shape=jax.ShapeDtypeStruct((128, 2048), bf16),
-        in_specs=[pl.BlockSpec(memory_space=pltpu.SMEM)] + [vmem] * 8 + [hbm]
-        + [vmem] * 4 + [hbm] * 2,
-        out_specs=vmem,
+        in_specs=[smem] * 2 + [hbm] * 18,
+        out_specs=pl.BlockSpec(memory_space=pltpu.VMEM),
         scratch_shapes=[
+            pltpu.VMEM((ROWS, 2048), bf16),
+            pltpu.VMEM((2048, 1024), bf16),
+            pltpu.VMEM((8, 2048), bf16),
+            pltpu.VMEM((1, 2048), f32),
+            pltpu.VMEM((1, ROWS), f32),
+            pltpu.VMEM((1, MD, MD), f32),
+            pltpu.VMEM((1, MD), f32),
+            pltpu.VMEM((1, 1024), f32),
+            pltpu.VMEM((1, 1024), f32),
+            pltpu.VMEM((2, AD, ROWS), bf16),
+            pltpu.VMEM((2, 2 * AD, ROWS), bf16),
+            pltpu.VMEM((MD, ROWS), bf16),
+            pltpu.VMEM((ROWS, MD), bf16),
+            pltpu.VMEM((MD, ROWS), bf16),
+            pltpu.VMEM((8, ROWS), f32),
+            pltpu.VMEM((8, ROWS), f32),
+            pltpu.VMEM((ROWS, 8), f32),
             pltpu.VMEM((1024, 2048), bf16),
             pltpu.VMEM((1024, 2048), bf16),
             pltpu.VMEM((N_SP, 2 * AD + 16, ROWS), bf16),
@@ -602,13 +662,13 @@
             pltpu.VMEM((N_TP, ZR, 128), bf16),
             pltpu.VMEM((ZR, ROWS), bf16),
             pltpu.VMEM((ZR, ROWS), f32),
-            dma((2,)), dma,
-            dma((8,)), dma((N_SP,)),
+            dma((20,)), dma((8,)),
+            dma((2,)), dma((N_SP,)),
             dma((2,)), dma((2,)),
             dma((N_SP,)), dma((N_SP,)),
             dma((N_TP,)), dma((N_TP,)),
             dma((2, N_TP)), dma((16,)),
-            dma((N_SP,)), dma, dma,
+            dma((4, 3)), dma((N_SP,)), dma, dma,
         ],
         compiler_params=pltpu.CompilerParams(
             collective_id=0, has_side_effects=True, vmem_limit_bytes=60 * 2**20
@@ -622,15 +682,11 @@
 def on_device(tokens, norm_gain, attn_query, attn_key, attn_value, score_scale, attention_decay,
               mem_query, mem_key, mem_value, mem_ingate, input_shift, memory_decay, mem_outgate,
               init_memory, init_normalizer, attn_gain, mem_gain, attn_out, mem_out):
-    q, kv, mq, mk, mv, mo, gate = project(
-        tokens, norm_gain.reshape(1, 2048),
-        (attn_query, attn_key, attn_value, mem_query, mem_key, mem_value, mem_outgate),
-        mem_ingate, input_shift.reshape(8, 1),
-    )
     return mix(
-        score_scale, q, kv, mq, mk, mv, mo, gate, memory_decay, attention_decay,
-        init_memory, init_normalizer, attn_gain.reshape(1, 1024), mem_gain.reshape(1, 1024),
-        attn_out, mem_out,
+        score_scale, input_shift, tokens, attn_query, attn_key, attn_value, mem_query, mem_key,
+        mem_value, mem_outgate, mem_ingate.T, norm_gain.reshape(1, 2048), memory_decay,
+        attention_decay, init_memory, init_normalizer, attn_gain.reshape(1, 1024),
+        mem_gain.reshape(1, 1024), attn_out, mem_out,
     )
 
 

time: 140 us -> 91 us (0.65)
  Pallas kernels: 122 us -> 89 us
  local copies, waits for them, and re-layouts: 16.6 us -> 1.88 us
    pallas_call x1, Pallas kernels: 113 us -> 89 us  [mix(): pl.pallas_call(mix_kernel, out_shape=jax.ShapeDtypeStruct((128, 2048), bf...]
    unnamed x32 -> x1, local copies, waits for them, and re-layouts: 15.8 us -> 1.88 us
    pallas_call x1 -> x0, Pallas kernels: 9.28 us -> none  [project(): pl.pallas_call(project_kernel, grid=(ROWS // tile,), in_specs=[pl.BlockSp...]
where the time goes in v2:
time: 91 us; the launch traced here: 90.9 us
  Pallas kernels  89 us (98%)
  local copies, waits for them, and re-layouts  1.88 us (2%)
    pallas_call x1, Pallas kernels, mix(): pl.pallas_call(mix_kernel, out_shape=jax.ShapeDtypeStruct((128, 2048), bf...  89 us
    unnamed x1, local copies, waits for them, and re-layouts  1.88 us

profile of v2, /device:TPU:1, one launch (start us, length us, event | category | flops | bytes accessed | tf_op | source)
XLA Modules:
  0.0 90.9 jit_solution(8090129779606563442)
XLA Ops:
  0.0 89.0 %shard_map.190 = bf16[128,2048]{1,0:T(8,128)(2,1)} custom-call(f32[16]{0:T(128)} %scale_ref.1, f32[8]{0:T(128)} %shift_ref.1, bf16[1024,2048]{1,0:T(8,128)(2,1)} %tok_in.1, bf16[2048,128]{1,0:T(8,128)(2,1)} %wq_in.1, bf16[2048,128]{1,0:T(8,128)(2,1)} %wk_in.1, bf16[2048,128]{1,0:T(8,128)(2,1)} %wv_in.1, bf16[2048,128]{1,0:T(8,128)(2,1)} %wmq_in.1, ...), custom_call_target="tpu_custom_call" | custom-call | flops 60000002048 | bytes 12582912 | tf_op jit(solution)/shard_map/pallas_call | solution.py:625
  89.0 1.9 %copy.22 = bf16[128,2048]{1,0:T(8,128)(2,1)} copy(bf16[128,2048]{1,0:T(8,128)(2,1)} %shard_map.190) | data formatting | bytes 1048576

commit v3 on v2

--- a/solution.py
+++ b/solution.py
@@ -19,6 +19,7 @@
 MD = 128
 QT = 256
 N_SP, N_TP = 16, 8
+RECALL_AT = 12
 VEXT = AD + 16
 ZR = MD + 16
 
@@ -66,23 +67,27 @@
                out, tok, w, ing, ngain, fade_in, cinit_in, ninit_in, again_in, mgain_in,
                qs, kvs, mq_in, mk_in, mo_in, fade_s, crest_s, levels,
                wa, wm, kv, qb, decays, kaug, qaug, best, acc, ostage, att,
-               zstage, zb, mstage, mb, mext, mnum,
+               zstage, zb, mstage, mb, mext, mnum, half,
                isem, wsem, kv_s, kv_r, q_s, q_r, z_s, z_r, m_s, m_r, o_s, o_r, p_s, f_s, d_s, d_r):
     r = lax.axis_index("sp")
     t = lax.axis_index("tp")
     x, k = t // 2, t % 2
     rz, ry = r // 4, r % 4
+
+    def member(z, y):
+        m = 2 * (z % 2) + y % 2
+        return jnp.where(z // 2 == 1, 3 - m, m)
+
     g = 2 * (rz // 2) + ry // 2
-    a = 2 * (rz % 2) + ry % 2
+    a = member(rz, ry)
     b = k
     hi = jnp.where(b == 0, 15 - a, 8 + a)
     lo = jnp.where(b == 0, a, 7 - a)
     head = 4 * x + g
 
     def chip_of(block, member):
-        z = 2 * (block // 2) + member // 2
-        y = 2 * (block % 2) + member % 2
-        return 4 * z + y
+        m = jnp.where(block // 2 == 1, 3 - member, member)
+        return 4 * (2 * (block // 2) + m // 2) + 2 * (block % 2) + m % 2
 
     def flip(v):
         return v + 1 - 2 * (v % 2)
@@ -186,17 +191,6 @@
             device_id=(sp, tp), device_id_type=MESH,
         )
 
-    for h in range(2):
-        own, copy = kv_copy(h)
-
-        @pl.when(jnp.logical_not(own))
-        def _():
-            copy.start()
-
-        @pl.when(own)
-        def _():
-            kv[r, 0 : 2 * AD] = kvs[h]
-
     def decay_copy():
         return pltpu.make_async_remote_copy(
             decay_in, decays.at[k], d_s, d_r, device_id=(r, 2 * x + 1 - k), device_id_type=MESH
@@ -213,6 +207,37 @@
         @pl.when(own)
         def _():
             qb[my_slot] = qs[h]
+
+    for h in range(2):
+        own, copy = kv_copy(h)
+
+        @pl.when(jnp.logical_not(own))
+        def _():
+            copy.start()
+
+        @pl.when(own)
+        def _():
+            kv[r, 0 : 2 * AD] = kvs[h]
+
+    def peer(p):
+        z = flip(rz) if p // 2 else rz
+        y = flip(ry) if p % 2 else ry
+        return 4 * z + y, member(z, y)
+
+    def block_copy(p):
+        chip, its_a = peer(p)
+        wanted = (g // 2 == k) & (r <= 15 - its_a)
+        return wanted, pltpu.make_async_remote_copy(
+            kvs.at[g % 2], kv.at[r, 0 : 2 * AD], p_s.at[0, p - 1], kv_r.at[r],
+            device_id=(chip, 2 * x + core_for(r)), device_id_type=MESH,
+        )
+
+    for p in (1, 2, 3):
+        wanted, copy = block_copy(p)
+
+        @pl.when(wanted)
+        def _():
+            copy.start()
 
     w[:, 896:1024] = jnp.zeros((2048, 128), bf16)
     w[:, 896:904] = ing[...].astype(f32).T.astype(bf16)
@@ -264,7 +289,10 @@
         return 0
 
     def chunk_at(n):
-        p, m = n // 4, n % 4
+        p = jnp.where(
+            n < 4, 0, jnp.where(n < 7, n - 3, jnp.where(n < 13, (n - 5) // 2, n - 12))
+        )
+        m = jnp.where(n < 4, n, jnp.where(n < 7, 0, jnp.where(n < 13, 1 + (n - 7) % 2, 3)))
         pz = jnp.where(p // 2 == 1, flip(rz), rz)
         py = jnp.where(p % 2 == 1, flip(ry), ry)
         cz = jnp.where(m // 2 == 1, 3 - pz, pz)
@@ -281,12 +309,10 @@
         )
 
     def peer_copy(chunk, n, p):
-        member = jnp.where(p // 2 == 1, 2 - 2 * (a // 2), 2 * (a // 2)) + jnp.where(
-            p % 2 == 1, 1 - a % 2, a % 2
-        )
-        return (chunk <= 15 - member), pltpu.make_async_remote_copy(
+        chip, its_a = peer(p)
+        return (chunk <= 15 - its_a), pltpu.make_async_remote_copy(
             kv.at[chunk, 0 : 2 * AD], kv.at[chunk, 0 : 2 * AD], p_s.at[n % 4, p - 1], kv_r.at[chunk],
-            device_id=(chip_of(g, member), t), device_id_type=MESH,
+            device_id=(chip, t), device_id_type=MESH,
         )
 
     def arrive(n, entry):
@@ -302,7 +328,7 @@
 
         @pl.when(reaches & mine)
         def _():
-            for p in (1, 2, 3) if entry else ():
+            for p in (1, 2, 3) if entry and n > 0 else ():
                 wanted, copy = peer_copy(chunk, n, p)
 
                 @pl.when(wanted)
@@ -312,10 +338,6 @@
             @pl.when(sibling_uses(chunk))
             def _():
                 forward_copy(chunk).start()
-
-    for n in range(4):
-        arrive(n, True)
-    lax.fori_loop(r + 1, N_SP, z_send, 0)
 
     for j in range(ROWS // QT):
         cols = slice(j * QT, j * QT + QT)
@@ -329,6 +351,8 @@
         p_hi, p_lo = halves(pair)
         mnum[:, cols] = dot(mext[:, 0:n_keys], p_hi) + dot(mext[:, 0:n_keys], p_lo)
 
+    arrive(0, True)
+
     w_copies = []
     for n in range(8):
         rows = slice(n % 4 * 256, n % 4 * 256 + 256)
@@ -372,21 +396,28 @@
 
     def fold(slot, chunk, diag):
         def scores(i):
-            n_keys = (i + 1) * QT if diag else ROWS
-            s = dot(kaug[0:n_keys], qaug[slot, :, i * QT : i * QT + QT])
-            if diag:
-                key_at = lax.broadcasted_iota(jnp.int32, (n_keys, QT), 0)
-                query_at = lax.broadcasted_iota(jnp.int32, (n_keys, QT), 1) + i * QT
-                s = jnp.where(key_at <= query_at, s, FAR)
-            return s
-
-        def finish(i, s):
             cols = slice(i * QT, i * QT + QT)
-            n_keys = s.shape[0]
+            out = []
+            for j in range(i + 1 if diag else ROWS // QT):
+                s = dot(kaug[j * QT : j * QT + QT], qaug[slot, :, cols])
+                if diag and j == i:
+                    key_at = lax.broadcasted_iota(jnp.int32, (QT, QT), 0)
+                    query_at = lax.broadcasted_iota(jnp.int32, (QT, QT), 1)
+                    s = jnp.where(key_at <= query_at, s, FAR)
+                out.append(s)
+            return out
+
+        def finish(i, parts):
+            cols = slice(i * QT, i * QT + QT)
             old = best[slot, 0:1, cols]
-            new = jnp.maximum(old, jnp.max(s, axis=0, keepdims=True))
-            weights = jnp.exp2(s - new).astype(bf16)
-            got = dot(kv[chunk, AD : AD + VEXT, 0:n_keys], weights)
+            tops = parts[0]
+            for s in parts[1:]:
+                tops = jnp.maximum(tops, s)
+            new = jnp.maximum(old, jnp.max(tops, axis=0, keepdims=True))
+            got = jnp.zeros((VEXT, QT), f32)
+            for j, s in enumerate(parts):
+                weights = jnp.exp2(s - new).astype(bf16)
+                got = got + dot(kv[chunk, AD : AD + VEXT, j * QT : j * QT + QT], weights)
             acc[slot, :, cols] = acc[slot, :, cols] * jnp.exp2(old - new) + got
             best[slot, 0:1, cols] = new
 
@@ -397,43 +428,60 @@
             finish(i, s)
             s = later
 
-    def visit(n, _):
-        @pl.when((n >= 3) & (n < 15))
-        def _():
-            arrive(n + 1, False)
-
-        chunk = chunk_at(n)
-
-        @pl.when(chunk <= hi)
-        def _():
-            take(chunk)
-
-        return 0
-
-    def take(chunk):
-        keys = kv[chunk, 0:AD]
-        keys32 = keys.astype(f32)
-        d_hi, d_mid, d_lo = pieces(decay_of(chunk))
-        extra = rows_of((d_hi, d_mid, d_lo, 1.0, 1.0, 1.0), 64, ROWS)
-        kaug[:, 0:128] = jnp.concatenate([keys32, extra], axis=0).T.astype(bf16)
-        kaug[:, 128:256] = jnp.concatenate([keys32, keys32], axis=0).T.astype(bf16)
-
-        def side(slot, _):
-            mine = jnp.where(slot == 0, hi, lo)
-
-            @pl.when(chunk < mine)
-            def _():
-                fold(slot, chunk, False)
-
-            @pl.when(chunk == mine)
-            def _():
-                fold(slot, chunk, True)
-
-            return 0
-
-        lax.fori_loop(0, 2, side, 0)
-
-    lax.fori_loop(0, 16, visit, 0)
+    def m_copy(p):
+        return pltpu.make_async_remote_copy(
+            mstage.at[p], mb.at[t], m_s.at[p], m_r.at[t], device_id=(r, p), device_id_type=MESH
+        )
+
+    def m_send(p, _):
+        @pl.when(p != t)
+        def _():
+            m_copy(p).start()
+
+        @pl.when(p == t)
+        def _():
+            mb[t] = mstage[p]
+
+        return 0
+
+    def recall():
+        z0 = jnp.concatenate(
+            [cinit_in[0].T, jnp.broadcast_to(ninit_in[...], (16, MD))], axis=0
+        )
+
+        def enter(n, carry):
+            state, log = carry
+            pltpu.make_async_remote_copy(
+                zstage, zb.at[n], z_s.at[0], z_r.at[n], device_id=(0, t), device_id_type=MESH
+            ).wait_recv()
+            rest = zb[n, MD:ZR].astype(f32)
+            norm = rest[0:1] + rest[1:2] + rest[2:3]
+            stab = rest[3:4] + rest[4:5] + rest[5:6]
+            faded = log + (rest[6:7] + rest[7:8] + rest[8:9])
+            new = jnp.maximum(faded, stab)
+            added = jnp.concatenate(
+                [zb[n, 0:MD].astype(f32), jnp.broadcast_to(norm, (16, MD))], axis=0
+            )
+            return state * jnp.exp(faded - new) + added * jnp.exp(stab - new), new
+
+        state, log = lax.fori_loop(0, r, enter, (z0, jnp.zeros((1, MD), f32)))
+        crest = crest_s[0:1]
+        log = log[:, 0:1]
+        peak = jnp.maximum(crest, log)
+        s_hi, s_lo = halves(state)
+        carried = (dot(s_hi, mq_in[...]) + dot(s_lo, mq_in[...])) * MD**-0.5
+        numer = mnum[...] * jnp.exp(crest - peak) + carried * jnp.exp(log - peak)
+        floor = jnp.exp(-(fade_s[0:1] + peak))
+        recalled = numer[0:MD] / jnp.maximum(jnp.abs(numer[MD : MD + 1]), floor)
+        squares = jnp.sum(recalled * recalled, axis=0, keepdims=True)
+        sq_hi, sq_mid, sq_lo = pieces(squares)
+        gated = (recalled * jax.nn.sigmoid(mo_in[...].astype(f32))).astype(bf16)
+        stats = rows_of((sq_hi, sq_mid, sq_lo), 16, ROWS).astype(bf16)
+        for p in range(N_TP):
+            mstage[p, 0:MD] = gated[:, p * 128 : p * 128 + 128]
+            mstage[p, MD:ZR] = stats[:, p * 128 : p * 128 + 128]
+
+        lax.fori_loop(0, N_TP, m_send, 0)
 
     def o_copy(slot, p):
         chunk = hi if slot == 0 else lo
@@ -443,7 +491,7 @@
             device_id=(chunk, p), device_id_type=MESH,
         )
 
-    for slot in range(2):
+    def depart(slot):
         result = acc[slot, 0:AD] / acc[slot, AD : AD + 1]
         result = result.astype(bf16)
         for p in range(N_TP):
@@ -464,59 +512,64 @@
 
         lax.fori_loop(0, N_TP, o_send, 0)
 
-    z0 = jnp.concatenate(
-        [cinit_in[0].T, jnp.broadcast_to(ninit_in[...], (16, MD))], axis=0
-    )
-
-    def enter(n, carry):
-        state, log = carry
-        pltpu.make_async_remote_copy(
-            zstage, zb.at[n], z_s.at[0], z_r.at[n], device_id=(0, t), device_id_type=MESH
-        ).wait_recv()
-        rest = zb[n, MD:ZR].astype(f32)
-        norm = rest[0:1] + rest[1:2] + rest[2:3]
-        stab = rest[3:4] + rest[4:5] + rest[5:6]
-        faded = log + (rest[6:7] + rest[7:8] + rest[8:9])
-        new = jnp.maximum(faded, stab)
-        added = jnp.concatenate(
-            [zb[n, 0:MD].astype(f32), jnp.broadcast_to(norm, (16, MD))], axis=0
-        )
-        return state * jnp.exp(faded - new) + added * jnp.exp(stab - new), new
-
-    state, log = lax.fori_loop(0, r, enter, (z0, jnp.zeros((1, MD), f32)))
-    crest = crest_s[0:1]
-    log = log[:, 0:1]
-    peak = jnp.maximum(crest, log)
-    s_hi, s_lo = halves(state)
-    carried = (dot(s_hi, mq_in[...]) + dot(s_lo, mq_in[...])) * MD**-0.5
-    numer = mnum[...] * jnp.exp(crest - peak) + carried * jnp.exp(log - peak)
-    floor = jnp.exp(-(fade_s[0:1] + peak))
-    recalled = numer[0:MD] / jnp.maximum(jnp.abs(numer[MD : MD + 1]), floor)
-    squares = jnp.sum(recalled * recalled, axis=0, keepdims=True)
-    sq_hi, sq_mid, sq_lo = pieces(squares)
-    gated = (recalled * jax.nn.sigmoid(mo_in[...].astype(f32))).astype(bf16)
-    stats = rows_of((sq_hi, sq_mid, sq_lo), 16, ROWS).astype(bf16)
-    for p in range(N_TP):
-        mstage[p, 0:MD] = gated[:, p * 128 : p * 128 + 128]
-        mstage[p, MD:ZR] = stats[:, p * 128 : p * 128 + 128]
-
-    def m_copy(p):
-        return pltpu.make_async_remote_copy(
-            mstage.at[p], mb.at[t], m_s.at[p], m_r.at[t], device_id=(r, p), device_id_type=MESH
-        )
-
-    def m_send(p, _):
-        @pl.when(p != t)
-        def _():
-            m_copy(p).start()
-
-        @pl.when(p == t)
-        def _():
-            mb[t] = mstage[p]
-
-        return 0
-
-    lax.fori_loop(0, N_TP, m_send, 0)
+    def visit(n, early):
+        @pl.when((n >= 3) & (n < 15))
+        def _():
+            arrive(n + 1, False)
+
+        chunk = chunk_at(n)
+
+        @pl.when(chunk <= hi)
+        def _():
+            take(chunk)
+
+        early = early + jnp.where(chunk <= lo, 1, 0)
+
+        @pl.when((chunk <= lo) & (early == lo + 1))
+        def _():
+            depart(1)
+
+        @pl.when(n == 0)
+        def _():
+            arrive(1, True)
+            arrive(2, True)
+
+        @pl.when(n == 1)
+        def _():
+            arrive(3, True)
+            lax.fori_loop(r + 1, N_SP, z_send, 0)
+
+        @pl.when(n == RECALL_AT)
+        def _():
+            recall()
+
+        return early
+
+    def take(chunk):
+        keys = kv[chunk, 0:AD]
+        d_hi, d_mid, d_lo = pieces(decay_of(chunk))
+        extra = rows_of((d_hi, d_mid, d_lo, 1.0, 1.0, 1.0), 64, ROWS)
+        kaug[:, 0:128] = jnp.concatenate([keys, extra.astype(bf16)], axis=0).T
+        kaug[:, 128:256] = jnp.concatenate([keys, keys], axis=0).T
+
+        def side(slot, _):
+            mine = jnp.where(slot == 0, hi, lo)
+
+            @pl.when(chunk < mine)
+            def _():
+                fold(slot, chunk, False)
+
+            @pl.when(chunk == mine)
+            def _():
+                fold(slot, chunk, True)
+
+            return 0
+
+        lax.fori_loop(0, 2, side, 0)
+
+    lax.fori_loop(0, 16, visit, 0)
+
+    depart(0)
 
     def o_wait(n, _):
         own = (n == head) & ((hi == r) | (lo == r))
@@ -548,6 +601,55 @@
     m_stats = sum(mb[n, MD:ZR].astype(f32) for n in range(N_TP)).T
     m_sq = m_stats[:, 0:1] + m_stats[:, 1:2] + m_stats[:, 2:3]
     m_mix = (m_all * lax.rsqrt(m_sq / 1024.0 + EPS) * mgain_in[...]).astype(bf16)
+
+    for n in range(4):
+        cols = slice(n * 512, n * 512 + 512)
+        half[:, cols] = dot(m_mix, wm[:, cols])
+
+    decay_copy().wait_send()
+    for h in range(2):
+        for own, copy in (q_copy(h), kv_copy(h)):
+
+            @pl.when(jnp.logical_not(own))
+            def _():
+                copy.wait_send()
+
+    for p in (1, 2, 3):
+        wanted, copy = block_copy(p)
+
+        @pl.when(wanted)
+        def _():
+            copy.wait_send()
+
+    def z_done(to, _):
+        z_copy(to).wait_send()
+        return 0
+
+    lax.fori_loop(r + 1, N_SP, z_done, 0)
+
+    def f_done(n, _):
+        chunk = chunk_at(n)
+        mine = core_for(chunk) == b
+        reaches = jnp.where(n < 4, True, chunk <= 15 - a)
+
+        @pl.when(reaches & mine)
+        def _():
+            @pl.when((n > 0) & (n < 4))
+            def _():
+                for p in (1, 2, 3):
+                    wanted, copy = peer_copy(chunk, n, p)
+
+                    @pl.when(wanted)
+                    def _():
+                        copy.wait_send()
+
+            @pl.when(sibling_uses(chunk))
+            def _():
+                forward_copy(chunk).wait_send()
+
+        return 0
+
+    lax.fori_loop(0, N_SP, f_done, 0)
 
     lax.fori_loop(0, 16, o_wait, 0)
     a_all = jnp.concatenate(
@@ -561,45 +663,7 @@
     a_mix = (a_all * lax.rsqrt(a_sq / 1024.0 + EPS) * again_in[...]).astype(bf16)
     for n in range(4):
         cols = slice(n * 512, n * 512 + 512)
-        out[:, cols] = (dot(m_mix, wm[:, cols]) + dot(a_mix, wa[:, cols])).astype(bf16)
-
-    decay_copy().wait_send()
-    for h in range(2):
-        for own, copy in (q_copy(h), kv_copy(h)):
-
-            @pl.when(jnp.logical_not(own))
-            def _():
-                copy.wait_send()
-
-    def z_done(to, _):
-        z_copy(to).wait_send()
-        return 0
-
-    lax.fori_loop(r + 1, N_SP, z_done, 0)
-
-    def f_done(n, _):
-        chunk = chunk_at(n)
-        mine = core_for(chunk) == b
-        reaches = jnp.where(n < 4, True, chunk <= 15 - a)
-
-        @pl.when(reaches & mine)
-        def _():
-            @pl.when(n < 4)
-            def _():
-                for p in (1, 2, 3):
-                    wanted, copy = peer_copy(chunk, n, p)
-
-                    @pl.when(wanted)
-                    def _():
-                        copy.wait_send()
-
-            @pl.when(sibling_uses(chunk))
-            def _():
-                forward_copy(chunk).wait_send()
-
-        return 0
-
-    lax.fori_loop(0, N_SP, f_done, 0)
+        out[:, cols] = (half[:, cols] + dot(a_mix, wa[:, cols])).astype(bf16)
 
     def p_done(p, _):
         for slot in range(2):
@@ -662,6 +726,7 @@
             pltpu.VMEM((N_TP, ZR, 128), bf16),
             pltpu.VMEM((ZR, ROWS), bf16),
             pltpu.VMEM((ZR, ROWS), f32),
+            pltpu.VMEM((128, 2048), f32),
             dma((20,)), dma((8,)),
             dma((2,)), dma((N_SP,)),
             dma((2,)), dma((2,)),

time: 91 us -> 78.6 us (0.86)
  the two profiles are of different devices: /device:TPU:1 before, /device:TPU:65 now
where the time goes in v3:
time: 78.6 us; the launch traced here: 78.5 us
  Pallas kernels  76.6 us (97%)
  local copies, waits for them, and re-layouts  1.88 us (2%)
    pallas_call x1, Pallas kernels, mix(): pl.pallas_call(mix_kernel, out_shape=jax.ShapeDtypeStruct((128, 2048), bf...  76.6 us
    unnamed x1, local copies, waits for them, and re-layouts  1.88 us

profile of v3, /device:TPU:65, one launch (start us, length us, event | category | flops | bytes accessed | tf_op | source)
XLA Modules:
  0.0 78.5 jit_solution(15024508088350248056)
XLA Ops:
  0.0 76.6 %shard_map.190 = bf16[128,2048]{1,0:T(8,128)(2,1)} custom-call(f32[16]{0:T(128)} %scale_ref.1, f32[8]{0:T(128)} %shift_ref.1, bf16[1024,2048]{1,0:T(8,128)(2,1)} %tok_in.1, bf16[2048,128]{1,0:T(8,128)(2,1)} %wq_in.1, bf16[2048,128]{1,0:T(8,128)(2,1)} %wk_in.1, bf16[2048,128]{1,0:T(8,128)(2,1)} %wv_in.1, bf16[2048,128]{1,0:T(8,128)(2,1)} %wmq_in.1, ...), custom_call_target="tpu_custom_call" | custom-call | flops 60000002048 | bytes 12582912 | tf_op jit(solution)/shard_map/pallas_call | solution.py:689
  76.6 1.9 %copy.22 = bf16[128,2048]{1,0:T(8,128)(2,1)} copy(bf16[128,2048]{1,0:T(8,128)(2,1)} %shard_map.190) | data formatting | bytes 1048576

commit v4 on v3

--- a/solution.py
+++ b/solution.py
@@ -19,6 +19,7 @@
 MD = 128
 QT = 256
 N_SP, N_TP = 16, 8
+ROW_AT = 7
 RECALL_AT = 12
 VEXT = AD + 16
 ZR = MD + 16
@@ -67,8 +68,8 @@
                out, tok, w, ing, ngain, fade_in, cinit_in, ninit_in, again_in, mgain_in,
                qs, kvs, mq_in, mk_in, mo_in, fade_s, crest_s, levels,
                wa, wm, kv, qb, decays, kaug, qaug, best, acc, ostage, att,
-               zstage, zb, mstage, mb, mext, mnum, half,
-               isem, wsem, kv_s, kv_r, q_s, q_r, z_s, z_r, m_s, m_r, o_s, o_r, p_s, f_s, d_s, d_r):
+               zstage, zb, rowstage, rowb, mstage, mb, mext, mnum, half,
+               isem, wsem, kv_s, kv_r, q_s, q_r, z_s, z_r, row_s, row_r, m_s, m_r, o_s, o_r, p_s, f_s, d_s, d_r):
     r = lax.axis_index("sp")
     t = lax.axis_index("tp")
     x, k = t // 2, t % 2
@@ -232,12 +233,15 @@
             device_id=(chip, 2 * x + core_for(r)), device_id_type=MESH,
         )
 
-    for p in (1, 2, 3):
+    def block_start(p):
         wanted, copy = block_copy(p)
 
         @pl.when(wanted)
         def _():
             copy.start()
+
+    block_start(1)
+    block_start(2)
 
     w[:, 896:1024] = jnp.zeros((2048, 128), bf16)
     w[:, 896:904] = ing[...].astype(f32).T.astype(bf16)
@@ -271,22 +275,72 @@
     weighted = mext[...].astype(f32) * jnp.exp(level[0:1] - top)
     w_hi, w_lo = halves(weighted)
     z = dot(w_hi, mk_in[...]) + dot(w_lo, mk_in[...])
-    zstage[0:MD] = z[0:MD].astype(bf16)
-    z_rest = (
-        *pieces(z[MD : MD + 1]),
-        *pieces(jnp.broadcast_to(total + top, (1, MD))),
-        *pieces(jnp.broadcast_to(total, (1, MD))),
-    )
-    zstage[MD:ZR] = rows_of(z_rest, 16, MD).astype(bf16)
+    def written(state, stab, faded):
+        packed = (
+            *pieces(state[MD : MD + 1]),
+            *pieces(jnp.broadcast_to(stab, (1, MD))),
+            *pieces(jnp.broadcast_to(faded, (1, MD))),
+        )
+        return jnp.concatenate([state[0:MD], rows_of(packed, 16, MD)], axis=0).astype(bf16)
+
+    def read(block):
+        rest = block[MD:ZR].astype(f32)
+        norm = rest[0:1] + rest[1:2] + rest[2:3]
+        state = jnp.concatenate(
+            [block[0:MD].astype(f32), jnp.broadcast_to(norm, (16, MD))], axis=0
+        )
+        return state, rest[3:4] + rest[4:5] + rest[5:6], rest[6:7] + rest[7:8] + rest[8:9]
+
+    def joined(state, log, block):
+        added, stab, faded = read(block)
+        log = log + faded
+        new = jnp.maximum(log, stab)
+        return state * jnp.exp(log - new) + added * jnp.exp(stab - new), new, faded
+
+    zstage[...] = written(z, total + top, total)
+    zb[ry] = zstage[...]
 
     def z_copy(to):
         return pltpu.make_async_remote_copy(
-            zstage, zb.at[r], z_s.at[to], z_r.at[r], device_id=(to, t), device_id_type=MESH
+            zstage, zb.at[ry], z_s.at[to], z_r.at[ry],
+            device_id=(4 * rz + to, t), device_id_type=MESH,
+        )
+
+    def row_copy(to):
+        return pltpu.make_async_remote_copy(
+            rowstage, rowb.at[rz], row_s.at[to], row_r.at[rz],
+            device_id=(4 * to + ry, t), device_id_type=MESH,
         )
 
     def z_send(to, _):
-        z_copy(to).start()
-        return 0
+        @pl.when(to != ry)
+        def _():
+            z_copy(to).start()
+
+        return 0
+
+    def row_send(to, _):
+        row_copy(to).start()
+        return 0
+
+    def row_total():
+        def take_in(n, _):
+            @pl.when(n != ry)
+            def _():
+                pltpu.make_async_remote_copy(
+                    zstage, zb.at[n], z_s.at[0], z_r.at[n],
+                    device_id=(4 * rz, t), device_id_type=MESH,
+                ).wait_recv()
+
+            return 0
+
+        lax.fori_loop(0, 4, take_in, 0)
+        state, stab, faded = read(zb[0])
+        for n in range(1, 4):
+            state, stab, more = joined(state, stab, zb[n])
+            faded = faded + more
+        rowstage[...] = written(state, stab, faded)
+        lax.fori_loop(rz + 1, 4, row_send, 0)
 
     def chunk_at(n):
         p = jnp.where(
@@ -328,16 +382,11 @@
 
         @pl.when(reaches & mine)
         def _():
-            for p in (1, 2, 3) if entry and n > 0 else ():
-                wanted, copy = peer_copy(chunk, n, p)
-
-                @pl.when(wanted)
-                def _():
-                    copy.start()
-
             @pl.when(sibling_uses(chunk))
             def _():
                 forward_copy(chunk).start()
+
+    lax.fori_loop(0, 4, z_send, 0)
 
     for j in range(ROWS // QT):
         cols = slice(j * QT, j * QT + QT)
@@ -351,7 +400,20 @@
         p_hi, p_lo = halves(pair)
         mnum[:, cols] = dot(mext[:, 0:n_keys], p_hi) + dot(mext[:, 0:n_keys], p_lo)
 
+    def push(n, peers):
+        chunk = chunk_at(n)
+        for p in peers:
+            wanted, copy = peer_copy(chunk, n, p)
+
+            @pl.when(wanted & (core_for(chunk) == b))
+            def _():
+                copy.start()
+
     arrive(0, True)
+    block_start(3)
+    for n in (1, 2):
+        arrive(n, True)
+        push(n, (1, 2))
 
     w_copies = []
     for n in range(8):
@@ -449,22 +511,18 @@
             [cinit_in[0].T, jnp.broadcast_to(ninit_in[...], (16, MD))], axis=0
         )
 
+        def enter_row(n, carry):
+            pltpu.make_async_remote_copy(
+                rowstage, rowb.at[n], row_s.at[0], row_r.at[n],
+                device_id=(ry, t), device_id_type=MESH,
+            ).wait_recv()
+            return joined(*carry, rowb[n])[:2]
+
         def enter(n, carry):
-            state, log = carry
-            pltpu.make_async_remote_copy(
-                zstage, zb.at[n], z_s.at[0], z_r.at[n], device_id=(0, t), device_id_type=MESH
-            ).wait_recv()
-            rest = zb[n, MD:ZR].astype(f32)
-            norm = rest[0:1] + rest[1:2] + rest[2:3]
-            stab = rest[3:4] + rest[4:5] + rest[5:6]
-            faded = log + (rest[6:7] + rest[7:8] + rest[8:9])
-            new = jnp.maximum(faded, stab)
-            added = jnp.concatenate(
-                [zb[n, 0:MD].astype(f32), jnp.broadcast_to(norm, (16, MD))], axis=0
-            )
-            return state * jnp.exp(faded - new) + added * jnp.exp(stab - new), new
-
-        state, log = lax.fori_loop(0, r, enter, (z0, jnp.zeros((1, MD), f32)))
+            return joined(*carry, zb[n])[:2]
+
+        carry = lax.fori_loop(0, rz, enter_row, (z0, jnp.zeros((1, MD), f32)))
+        state, log = lax.fori_loop(0, ry, enter, carry)
         crest = crest_s[0:1]
         log = log[:, 0:1]
         peak = jnp.maximum(crest, log)
@@ -512,16 +570,19 @@
 
         lax.fori_loop(0, N_TP, o_send, 0)
 
-    def visit(n, early):
-        @pl.when((n >= 3) & (n < 15))
-        def _():
-            arrive(n + 1, False)
-
+    def next_one(j, _):
+        arrive(j, False)
+        return 0
+
+    def visit(n, carry):
+        early, ahead = carry
+        lax.fori_loop(ahead, n + 1, next_one, 0)
+        ahead = jnp.maximum(ahead, n + 1)
         chunk = chunk_at(n)
 
         @pl.when(chunk <= hi)
         def _():
-            take(chunk)
+            take(chunk, n, ahead)
 
         early = early + jnp.where(chunk <= lo, 1, 0)
 
@@ -531,21 +592,30 @@
 
         @pl.when(n == 0)
         def _():
-            arrive(1, True)
-            arrive(2, True)
+            push(1, (3,))
+            push(2, (3,))
+            arrive(3, True)
 
         @pl.when(n == 1)
         def _():
-            arrive(3, True)
-            lax.fori_loop(r + 1, N_SP, z_send, 0)
+            push(3, (1, 2))
+
+        @pl.when(n == 2)
+        def _():
+            push(3, (3,))
+
+        @pl.when(n == ROW_AT)
+        def _():
+            row_total()
 
         @pl.when(n == RECALL_AT)
         def _():
             recall()
 
-        return early
-
-    def take(chunk):
+        folds = jnp.where(chunk <= hi, 1, 0) + jnp.where(chunk <= lo, 1, 0)
+        return early, jnp.minimum(ahead + jnp.where(n >= 2, folds, 0), N_SP)
+
+    def take(chunk, n, ahead):
         keys = kv[chunk, 0:AD]
         d_hi, d_mid, d_lo = pieces(decay_of(chunk))
         extra = rows_of((d_hi, d_mid, d_lo, 1.0, 1.0, 1.0), 64, ROWS)
@@ -563,11 +633,15 @@
             def _():
                 fold(slot, chunk, True)
 
+            @pl.when((chunk <= mine) & (n >= 2) & (ahead + slot < N_SP))
+            def _():
+                arrive(ahead + slot, False)
+
             return 0
 
         lax.fori_loop(0, 2, side, 0)
 
-    lax.fori_loop(0, 16, visit, 0)
+    lax.fori_loop(0, 16, visit, (0, 4))
 
     depart(0)
 
@@ -622,10 +696,18 @@
             copy.wait_send()
 
     def z_done(to, _):
-        z_copy(to).wait_send()
-        return 0
-
-    lax.fori_loop(r + 1, N_SP, z_done, 0)
+        @pl.when(to != ry)
+        def _():
+            z_copy(to).wait_send()
+
+        return 0
+
+    def row_done(to, _):
+        row_copy(to).wait_send()
+        return 0
+
+    lax.fori_loop(0, 4, z_done, 0)
+    lax.fori_loop(rz + 1, 4, row_done, 0)
 
     def f_done(n, _):
         chunk = chunk_at(n)
@@ -721,7 +803,9 @@
             pltpu.VMEM((2, N_TP, AD, 128), bf16),
             pltpu.VMEM((16, AD, 128), bf16),
             pltpu.VMEM((ZR, MD), bf16),
-            pltpu.VMEM((N_SP, ZR, MD), bf16),
+            pltpu.VMEM((4, ZR, MD), bf16),
+            pltpu.VMEM((ZR, MD), bf16),
+            pltpu.VMEM((4, ZR, MD), bf16),
             pltpu.VMEM((N_TP, ZR, 128), bf16),
             pltpu.VMEM((N_TP, ZR, 128), bf16),
             pltpu.VMEM((ZR, ROWS), bf16),
@@ -730,7 +814,7 @@
             dma((20,)), dma((8,)),
             dma((2,)), dma((N_SP,)),
             dma((2,)), dma((2,)),
-            dma((N_SP,)), dma((N_SP,)),
+            dma((4,)), dma((4,)), dma((4,)), dma((4,)),
             dma((N_TP,)), dma((N_TP,)),
             dma((2, N_TP)), dma((16,)),
             dma((4, 3)), dma((N_SP,)), dma, dma,

time: 78.6 us -> 78 us (level)
  Pallas kernels: 76.6 us -> 75.7 us
    pallas_call x1, Pallas kernels: 76.6 us -> 75.7 us  [mix(): pl.pallas_call(mix_kernel, out_shape=jax.ShapeDtypeStruct((128, 2048), bf...]
where the time goes in v4:
time: 78 us; the launch traced here: 77.6 us
  Pallas kernels  75.7 us (97%)
  local copies, waits for them, and re-layouts  1.88 us (2%)
    pallas_call x1, Pallas kernels, mix(): pl.pallas_call(mix_kernel, out_shape=jax.ShapeDtypeStruct((128, 2048), bf...  75.7 us
    unnamed x1, local copies, waits for them, and re-layouts  1.88 us

profile of v4, /device:TPU:65, one launch (start us, length us, event | category | flops | bytes accessed | tf_op | source)
XLA Modules:
  0.0 77.6 jit_solution(4814208576607475457)
XLA Ops:
  0.0 75.7 %shard_map.190 = bf16[128,2048]{1,0:T(8,128)(2,1)} custom-call(f32[16]{0:T(128)} %scale_ref.1, f32[8]{0:T(128)} %shift_ref.1, bf16[1024,2048]{1,0:T(8,128)(2,1)} %tok_in.1, bf16[2048,128]{1,0:T(8,128)(2,1)} %wq_in.1, bf16[2048,128]{1,0:T(8,128)(2,1)} %wk_in.1, bf16[2048,128]{1,0:T(8,128)(2,1)} %wv_in.1, bf16[2048,128]{1,0:T(8,128)(2,1)} %wmq_in.1, ...), custom_call_target="tpu_custom_call" | custom-call | flops 60000002048 | bytes 12582912 | tf_op jit(solution)/shard_map/pallas_call | solution.py:771
  75.7 1.9 %copy.22 = bf16[128,2048]{1,0:T(8,128)(2,1)} copy(bf16[128,2048]{1,0:T(8,128)(2,1)} %shard_map.190) | data formatting | bytes 1048576

commit v5 on v4

--- a/solution.py
+++ b/solution.py
@@ -411,9 +411,6 @@
 
     arrive(0, True)
     block_start(3)
-    for n in (1, 2):
-        arrive(n, True)
-        push(n, (1, 2))
 
     w_copies = []
     for n in range(8):
@@ -592,12 +589,15 @@
 
         @pl.when(n == 0)
         def _():
+            for entry in (1, 2):
+                arrive(entry, True)
+                push(entry, (1, 2))
+
+        @pl.when(n == 1)
+        def _():
             push(1, (3,))
             push(2, (3,))
             arrive(3, True)
-
-        @pl.when(n == 1)
-        def _():
             push(3, (1, 2))
 
         @pl.when(n == 2)

time: 78 us -> 75.6 us (0.969)
  Pallas kernels: 75.7 us -> 73.2 us
    pallas_call x1, Pallas kernels: 75.7 us -> 73.2 us  [mix(): pl.pallas_call(mix_kernel, out_shape=jax.ShapeDtypeStruct((128, 2048), bf...]
where the time goes in v5:
time: 75.6 us; the launch traced here: 75.1 us
  Pallas kernels  73.2 us (97%)
  local copies, waits for them, and re-layouts  1.88 us (2%)
    pallas_call x1, Pallas kernels, mix(): pl.pallas_call(mix_kernel, out_shape=jax.ShapeDtypeStruct((128, 2048), bf...  73.2 us
    unnamed x1, local copies, waits for them, and re-layouts  1.88 us

profile of v5, /device:TPU:65, one launch (start us, length us, event | category | flops | bytes accessed | tf_op | source)
XLA Modules:
  0.0 75.1 jit_solution(17721822174601871955)
XLA Ops:
  0.0 73.2 %shard_map.190 = bf16[128,2048]{1,0:T(8,128)(2,1)} custom-call(f32[16]{0:T(128)} %scale_ref.1, f32[8]{0:T(128)} %shift_ref.1, bf16[1024,2048]{1,0:T(8,128)(2,1)} %tok_in.1, bf16[2048,128]{1,0:T(8,128)(2,1)} %wq_in.1, bf16[2048,128]{1,0:T(8,128)(2,1)} %wk_in.1, bf16[2048,128]{1,0:T(8,128)(2,1)} %wv_in.1, bf16[2048,128]{1,0:T(8,128)(2,1)} %wmq_in.1, ...), custom_call_target="tpu_custom_call" | custom-call | flops 60000002048 | bytes 12582912 | tf_op jit(solution)/shard_map/pallas_call | solution.py:771
  73.2 1.9 %copy.22 = bf16[128,2048]{1,0:T(8,128)(2,1)} copy(bf16[128,2048]{1,0:T(8,128)(2,1)} %shard_map.190) | data formatting | bytes 1048576
